TPU v7x, 32 devices: a whole 2x2x4 slice. The times are simulated.
32 devices in a mesh: sp: 8 (over z, x), tp: 4 (over y, core).
Axes of the slice: x: 2, y: 2, z: 4, core: 2. Of those that a mesh axis runs over, the one named last changes fastest.
Arguments:
- prompt_tokens: bfloat16 [8192, 2048], P(('sp', 'tp')), may hold values from -8 to 8
- key_weight: bfloat16 [2048, 2048], P(None, 'tp'), may hold values from -0.125 to 0.125
- value_weight: bfloat16 [2048, 4096], P(None, 'tp'), may hold values from -0.125 to 0.125
- input_weight: bfloat16 [2048, 32], replicated, may hold values from -4 to 4
- forget_weight: bfloat16 [2048, 32], replicated, may hold values from -0.125 to 0.125
- forget_bias: float32 [32], replicated, as said below
- new_token: bfloat16 [2048], replicated, may hold values from -8 to 8
- new_query: bfloat16 [2048], P('tp'), may hold values from -6 to 6
Outputs:
- key_cache: bfloat16 [8192, 2048], P('sp', 'tp')
- value_cache: bfloat16 [8192, 4096], P('sp', 'tp')
- cache_weight: float32 [32, 8192], P('tp', 'sp')
- reading: float32 [4096], P('tp')
Inputs may be any that keep to these rules, and one draw needn't show every extreme that they name: `forget_bias`: every head's forget gate offset is 2 or more.
All inputs are finite; a program needn't handle non-finite values.
Results may differ from a plain program's by a relative error of at most 0.0058.
Values may be sent and summed in bfloat16 or wider, within the bound.
No kernel may reach another device: no remote copies, remote signals or barrier semaphores. Data moves between devices by JAX's collectives and lax.ppermute only.
A program may use at most 64 MiB of HBM per device.

v0:
```python
import math

import jax
import jax.numpy as jnp
from jax import lax
from jax.sharding import PartitionSpec as P

DQK = 64
DV = 128


def prefix(array, axis, combine, identity):
    peers, here = (lax.axis_size(axis), lax.axis_index(axis))
    everything = lax.all_gather(array, axis)
    start = jnp.broadcast_to(jnp.asarray(identity, array.dtype), array.shape)

    def step(k, before):
        at = peers - 1 - k
        reached = at > here
        new = combine(before, everything[at])
        return jnp.where(reached, new, before)

    return lax.fori_loop(0, peers, step, start)


def add_pairs(earlier, later_part):
    return earlier + later_part


def body(
    prompt_tokens,
    key_weight,
    value_weight,
    input_weight,
    forget_weight,
    forget_bias,
    new_token,
    new_query,
):
    heads_dev = key_weight.shape[1] // DQK
    head_start = lax.axis_index("tp") * heads_dev
    gate_input = lax.dynamic_slice_in_dim(input_weight, head_start, heads_dev, 1)
    gate_forget = lax.dynamic_slice_in_dim(forget_weight, head_start, heads_dev, 1)
    forget_shift = lax.dynamic_slice_in_dim(forget_bias, head_start, heads_dev, 0)
    packed = jnp.concatenate([key_weight, value_weight, gate_input, gate_forget], axis=1)
    key_end = heads_dev * DQK
    value_end = heads_dev * (DQK + DV)
    projected = jnp.dot(
        lax.all_gather(prompt_tokens, "tp", axis=0, tiled=True),
        packed,
        preferred_element_type=jnp.float32,
    )
    key_cache = projected[:, :key_end].astype(jnp.bfloat16)
    value_cache = projected[:, key_end:value_end].astype(jnp.bfloat16)
    input_gate = projected[:, value_end : value_end + heads_dev]
    forget_pre = projected[:, value_end + heads_dev :]
    log_forget = jax.nn.log_sigmoid(forget_pre + forget_shift)
    block_total = jnp.sum(log_forget, axis=0)
    carried = prefix(block_total, "sp", add_pairs, jnp.zeros_like(block_total))
    log_weight = (
        input_gate + (block_total[None, :] - jnp.cumsum(log_forget, axis=0)) + carried[None, :]
    )
    peak_log = lax.pmax(jnp.max(log_weight, axis=0), "sp")
    cache_weight = jnp.transpose(jnp.exp(log_weight - peak_log[None, :]), (1, 0))
    new_key = jnp.dot(new_token, key_weight, preferred_element_type=jnp.float32).astype(
        jnp.bfloat16
    )
    new_value = jnp.dot(new_token, value_weight, preferred_element_type=jnp.float32).astype(
        jnp.bfloat16
    )
    new_gate = jnp.dot(new_token, gate_input, preferred_element_type=jnp.float32)
    new_forget = jax.nn.log_sigmoid(
        jnp.dot(new_token, gate_forget, preferred_element_type=jnp.float32) + forget_shift
    )
    stable_level = jnp.maximum(new_forget + peak_log, new_gate)
    rows = log_weight.shape[0]
    query_heads = new_query.reshape(heads_dev, DQK)
    key_heads = key_cache.reshape(rows, heads_dev, DQK)
    key_score = jnp.einsum(
        "shd,hd->sh", key_heads, query_heads, preferred_element_type=jnp.float32
    ) / math.sqrt(DQK)
    new_score = jnp.einsum(
        "hd,hd->h", new_key.reshape(heads_dev, DQK), query_heads, preferred_element_type=jnp.float32
    ) / math.sqrt(DQK)
    weighted = jnp.exp(new_forget[None, :] + log_weight - stable_level[None, :]) * key_score
    value_heads = value_cache.reshape(rows, heads_dev, DV)
    numer_part = jnp.einsum(
        "sh,she->he", weighted.astype(jnp.bfloat16), value_heads, preferred_element_type=jnp.float32
    )
    denom_part = jnp.sum(weighted, axis=0)
    numerator, denominator = lax.psum((numer_part, denom_part), "sp")
    own_term = jnp.exp(new_gate - stable_level) * new_score
    numerator = numerator + own_term[:, None] * new_value.reshape(heads_dev, DV).astype(jnp.float32)
    denominator = denominator + own_term
    reading = numerator / jnp.maximum(jnp.abs(denominator), 1.0)[:, None]
    return (key_cache, value_cache, cache_weight, reading.reshape(-1))


def solution(mesh):
    placed = (P(("sp", "tp"), None), P(None, "tp"), P(None, "tp"), P(), P(), P(), P(), P("tp"))
    return jax.shard_map(
        body,
        mesh=mesh,
        in_specs=placed,
        out_specs=(P("sp", "tp"), P("sp", "tp"), P("tp", "sp"), P("tp")),
        check_vma=False,
    )
```

profile of v0, /device:TPU:0, one launch (start us, length us, event | category | flops | bytes accessed | tf_op | source)
XLA Modules:
  0.0 138.1 jit_solution(2018318325805021415)
XLA Ops:
  7.2 0.0 copy-start.2
  7.2 0.0 copy-start
  7.2 0.0 all-gather.3.cloned.1.call-start
  7.2 0.7 all-gather.3.cloned.1.call-update
  7.9 0.8 reshape.54
  8.7 0.8 reshape.80
  9.5 0.7 reshape.65
  10.2 2.0 %fusion.20 = f32[1,512]{1,0:T(1,128)S(1)} fusion(bf16[2048,1]{0,1:T(2,128)(2,1)S(1)} %reshape.65, bf16[2048,512]{1,0:T(8,128)(2,1)} %param.11), kind=kOutput, calls=%fused_computation.43 | convolution fusion | flops 2097152 | bytes 2103296 | tf_op jit(solution)/shard_map/dot_general | solution.py:65
  12.1 0.1 reshape.56
  12.2 0.7 dynamic_slice.21
  13.0 0.8 constant_dynamic-slice_fusion
  13.7 0.3 copy.18
  14.0 0.3 copy.17
  14.3 0.0 copy-done.2
  14.3 0.6 dynamic-slice
  15.5 0.0 copy-done
  15.5 10.7 %concatenate.3 = bf16[2048,1552]{1,0:T(8,128)(2,1)} concatenate(bf16[2048,512]{1,0:T(8,128)(2,1)S(1)} %copy-done, bf16[2048,1024]{1,0:T(8,128)(2,1)} %param.12, bf16[2048,8]{1,0:T(8,128)(2,1)S(1)} %copy.17, bf16[2048,8]{1,0:T(8,128)(2,1)S(1)} %copy.18), dimensions={1} | concatenate | bytes 12713984 | tf_op jit(solution)/shard_map/concatenate | solution.py:45
  26.2 0.1 fusion.11
  26.3 0.1 fusion.13
  26.5 2.8 %fusion.21 = f32[1,1024]{1,0:T(1,128)S(1)} fusion(bf16[2048,1]{0,1:T(2,128)(2,1)S(1)} %reshape.65, bf16[2048,1024]{1,0:T(8,128)(2,1)} %param.12), kind=kOutput, calls=%fused_computation.44 | convolution fusion | flops 4194304 | bytes 4202496 | tf_op jit(solution)/shard_map/dot_general | solution.py:68
  29.3 17.5 %all-gather.3.cloned.1.call-done = bf16[1024,2048]{1,0:T(8,128)(2,1)} async-done(((bf16[256,2048]{1,0:T(8,128)(2,1)}), bf16[1024,2048]{1,0:T(8,128)(2,1)}) %all-gather.3.cloned.1.call-update) | async-done | bytes 4194320 | tf_op jit(solution)/shard_map/all_gather | solution.py:49
  46.8 13.5 %fusion.18 = (bf16[1024,1552]{0,1:T(8,128)(2,1)S(1)}, f32[1024,1552]{0,1:T(8,128)S(1)}) fusion(bf16[2048,1552]{1,0:T(8,128)(2,1)} %concatenate.3, bf16[1024,2048]{1,0:T(8,128)(2,1)} %all-gather.3.cloned.1.call-done), kind=kOutput, calls=%fused_computation.41 | convolution fusion | flops 6511149056 | bytes 20086784 | tf_op jit(solution)/shard_map/dot_general | solution.py:48
  60.3 0.0 copy-start.1
  60.3 0.1 slice.26
  60.4 0.2 slice.27
  60.5 0.2 negate_bitcast_fusion
  60.7 2.2 %copy-done.1 = f32[1024,1552]{0,1:T(8,128)} copy-done((f32[1024,1552]{0,1:T(8,128)}, f32[1024,1552]{0,1:T(8,128)S(1)}, u32[]{:S(2)}) %copy-start.1) | copy-done | bytes 6357016
  62.9 2.3 %reduce-window.6 = f32[8,8,128]{2,1,0:T(8,128)S(1)} reduce-window(f32[8,8,128]{2,1,0:T(8,128)S(1)} %copy.19, f32[]{:T(128)} %constant.72.clone.1), window={size=1x1x128 pad=0_0x0_0x127_0}, to_apply=%region_1.2 | reduce-window | flops 1040384 | bytes 65540 | tf_op jit(solution)/shard_map/reduce-window
  65.2 0.1 fusion.17
  65.3 21.3 %all-reduce = f32[64]{0:T(128)S(1)} all-reduce(f32[64]{0:T(128)S(1)} %get-tuple-element.158), channel_id=2, replica_groups=mesh['sp'=8,'tp'=4] {'sp'}, use_global_device_ids=true, to_apply=%add | all-reduce | flops 64 | bytes 512
  86.6 0.1 reshape.59
  86.7 0.3 while.16
  87.1 0.2 slice_reduce_fusion
  87.2 0.2 reduce-window.9
  87.4 0.1 add_bitcast_fusion
  87.4 1.0 fusion.15
  88.4 17.1 %pmax.7 = f32[8]{0:T(128)S(1)} all-reduce(f32[8]{0:T(128)S(1)} %get-tuple-element.150), channel_id=1, replica_groups=mesh['sp'=8,'tp'=4] {'sp'}, use_global_device_ids=true, to_apply=%region_6.7 | all-reduce | flops 8 | bytes 64 | tf_op jit(solution)/shard_map/pmax | solution.py:63
  105.5 1.3 copy.20
  106.8 2.5 %copy.21 = bf16[1024,1024]{1,0:T(8,128)(2,1)} copy(bf16[1024,1024]{0,1:T(8,128)(2,1)S(1)} %slice.27) | data formatting | bytes 4194304
  109.4 0.1 add_maximum_fusion
  109.5 0.3 fusion.19
  109.8 0.8 fusion.14
  110.6 0.6 fusion.6
  111.2 19.4 %all-reduce.1 = (f32[8,128]{1,0:T(8,128)S(1)}, f32[8]{0:T(128)S(1)}) all-reduce(f32[8,128]{1,0:T(8,128)S(1)} %bitcast.85, f32[8]{0:T(128)S(1)} %get-tuple-element.154), channel_id=1, replica_groups=mesh['sp'=8,'tp'=4] {'sp'}, use_global_device_ids=true, to_apply=%region_7.8 | all-reduce | flops 1032 | bytes 8256 | tf_op jit(solution)/shard_map/psum | solution.py:91
  130.6 0.7 fusion.10
  (13 shorter events, 0.2 us)
Async XLA Ops:
  7.2 7.1 %copy-start.2 = (u32[32]{0:T(128)S(1)}, u32[32]{0:T(128)}, u32[]{:S(2)}) copy-start(u32[32]{0:T(128)} %constant.80) | copy-start | bytes 388
  7.2 8.4 %copy-start = (bf16[2048,512]{1,0:T(8,128)(2,1)S(1)}, bf16[2048,512]{1,0:T(8,128)(2,1)}, u32[]{:S(2)}) copy-start(bf16[2048,512]{1,0:T(8,128)(2,1)} %param.11) | copy-start | bytes 6291460
  7.2 39.6 %all-gather.3.cloned.1.call-start = ((), (), s32[]{:S(2)}) async-start(), calls=%async_computation | async-start | bytes 5242880 | tf_op jit(solution)/shard_map/all_gather | solution.py:49
  60.3 2.7 %copy-start.1 = (f32[1024,1552]{0,1:T(8,128)}, f32[1024,1552]{0,1:T(8,128)S(1)}, u32[]{:S(2)}) copy-start(f32[1024,1552]{0,1:T(8,128)S(1)} %get-tuple-element.160) | copy-start | bytes 19070980
Sparse Core Ops, SparseCore 0:
  9.6 37.1 all-gather.2
where the time goes:
time: 139 us; the launch traced here: 138 us
  blocking collectives  57.8 us (42%)
  local copies, waits for them, and re-layouts  22.2 us (16%)
  matrix products  19.5 us (14%)
  waiting for transfers between devices  18.1 us (13%)
  between operations  14.8 us (11%)
  other arithmetic  5.51 us (4%)
    unnamed x1, blocking collectives  21.3 us
    psum x1, blocking collectives, body(): numerator, denominator = lax.psum((numer_part, denom_part), 'sp')  19.4 us
    all_gather x1, waiting for transfers between devices, body(): lax.all_gather(prompt_tokens, 'tp', axis=0, tiled=True)  17.5 us
    pmax x1, blocking collectives, body(): peak_log = lax.pmax(jnp.max(log_weight, axis=0), 'sp')  17.1 us
    dot_general x1, matrix products, body(): jnp.dot(lax.all_gather(prompt_tokens, 'tp', axis=0, tiled=True), packed,...  13.5 us
    concatenate x1, local copies, waits for them, and re-layouts, body(): jnp.concatenate([key_weight, value_weight, gate_input, gate_forget], axis=1)  10.7 us
    unnamed x11, local copies, waits for them, and re-layouts  7.33 us
    dot_general x1, matrix products, body(): jnp.dot(new_token, value_weight, preferred_element_type=jnp.float32)  2.85 us
  transfers between devices with their start and end apart: 1, of which 1 were waited for; matrix products, arithmetic and copies ran while one was open for 15% of the time, Pallas kernels for 0%

commit v1 on v0

v1 whole, which is shorter than its diff:
```python
import functools
import math

import jax
import jax.numpy as jnp
from jax import lax
from jax.experimental import pallas as pl
from jax.experimental.pallas import tpu as pltpu
from jax.sharding import PartitionSpec as P


DQK = 64
DV = 128
LANES = 128
F32 = jnp.float32
BF16 = jnp.bfloat16

TOTAL, PEAK, DENOM, CARRIED = 0, 1, 2, 3
NEW_GATE, NEW_FORGET, NEW_SCORE = 4, 5, 6


def params(mib=24):
    return pltpu.CompilerParams(vmem_limit_bytes=mib * 1024 * 1024)


def cost(flops, moved):
    return pl.CostEstimate(flops=int(flops), bytes_accessed=int(moved), transcendentals=0)


def vmem():
    return pl.BlockSpec(memory_space=pltpu.VMEM)


def log_sigmoid(x):
    z = jnp.exp(-jnp.abs(x))
    u = 1.0 + z
    log1p = jnp.where(u == 1.0, z, jnp.log(u) * z / jnp.where(u == 1.0, 1.0, u - 1.0))
    return jnp.minimum(x, 0.0) - log1p


def lane_pack(values, rows):
    lane = lax.broadcasted_iota(jnp.int32, (rows, LANES), 1)
    out = jnp.zeros((rows, LANES), F32)
    for at, value in values.items():
        out = jnp.where(lane == at, value, out)
    return out


def nt_dot(a, b):
    return lax.dot_general(a, b, (((1,), (1,)), ((), ())), preferred_element_type=F32)


def carries(totals):
    out, running = [], jnp.zeros_like(totals[0])
    for total in reversed(totals):
        out.append(running)
        running = running + total
    return out[::-1], running


def column(stats, at):
    return stats[:, at : at + 1]


def merge(slots, mine, heads):
    radix = slots.shape[0]
    stats = [slots[k, :, DV:] for k in range(radix)]
    totals = [column(s, TOTAL) for s in stats]
    carry, total = carries(totals)
    peaks = [column(s, PEAK) + c for s, c in zip(stats, carry, strict=True)]
    peak = functools.reduce(jnp.maximum, peaks)
    numer = jnp.zeros((heads, DV), F32)
    denom = jnp.zeros((heads, 1), F32)
    after = jnp.zeros((heads, 1), F32)
    for k in range(radix):
        scale = jnp.exp(peaks[k] - peak)
        numer = numer + scale * slots[k, :, :DV]
        denom = denom + scale * column(stats[k], DENOM)
        after = after + jnp.where(mine == k, carry[k], 0.0)
    return numer, denom, total, peak, after


def place(slots, message_refs, digit):
    for k, ref in enumerate(message_refs):
        slots[digit ^ k] = ref[...]


def merge_kernel(heads, radix, stride, *refs):
    message_refs, out_ref, slots = refs[:radix], refs[radix], refs[radix + 1]
    digit = lax.rem(lax.axis_index("sp") // stride, radix)
    place(slots, message_refs, digit)
    numer, denom, total, peak, after = merge(slots, digit, heads)
    carried = message_refs[0][:, DV + CARRIED : DV + CARRIED + 1] + after
    out_ref[:, :DV] = numer
    out_ref[:, DV:] = lane_pack(
        {TOTAL: total, PEAK: peak, DENOM: denom, CARRIED: carried}, heads
    )


def finish_kernel(heads, radix, stride, *refs):
    message_refs = refs[:radix]
    kept_ref, log_ref, weight_ref, reading_ref, slots = refs[radix:]
    digit = lax.rem(lax.axis_index("sp") // stride, radix)
    place(slots, message_refs, digit)
    numer, denom, _, peak, after = merge(slots, digit, heads)
    carried = message_refs[0][:, DV + CARRIED : DV + CARRIED + 1] + after
    new = kept_ref[:, DV:]
    new_gate, new_forget = column(new, NEW_GATE), column(new, NEW_FORGET)
    stable = jnp.maximum(new_forget + peak, new_gate)
    scale = jnp.exp(new_forget + peak - stable)
    own_term = jnp.exp(new_gate - stable) * column(new, NEW_SCORE)
    numerator = numer * scale + own_term * kept_ref[:, :DV]
    denominator = denom * scale + own_term
    reading_ref[...] = numerator / jnp.maximum(jnp.abs(denominator), 1.0)
    weight_ref[...] = jnp.exp(log_ref[...] + (carried - peak))


def to_stage(message, flip, peers):
    return lax.ppermute(message, "sp", [(i, i ^ flip) for i in range(peers)])


def exchange(message, kept, log_weight, peers):
    heads, width = message.shape
    radices, left = [], peers
    while left > 1:
        radices.append(4 if left % 4 == 0 and (left // 4 == 1 or radices) else 2)
        left //= radices[-1]
    stride = 1
    for n, radix in enumerate(radices):
        others = [to_stage(message, k * stride, peers) for k in range(1, radix)]
        slots = [pltpu.VMEM((radix, heads, width), F32)]
        if n < len(radices) - 1:
            message = pl.pallas_call(
                functools.partial(merge_kernel, heads, radix, stride),
                out_shape=jax.ShapeDtypeStruct(message.shape, F32),
                in_specs=[vmem()] * radix,
                out_specs=vmem(),
                scratch_shapes=slots,
                compiler_params=params(4),
                cost_estimate=cost(1e6, 1e5),
                name="merge",
            )(message, *others)
        else:
            return pl.pallas_call(
                functools.partial(finish_kernel, heads, radix, stride),
                out_shape=(
                    jax.ShapeDtypeStruct(log_weight.shape, F32),
                    jax.ShapeDtypeStruct((heads, DV), F32),
                ),
                in_specs=[vmem()] * (radix + 2),
                out_specs=(vmem(), vmem()),
                scratch_shapes=slots,
                compiler_params=params(4),
                cost_estimate=cost(1e6, 1e5),
                name="finish",
            )(message, *others, kept, log_weight)
        stride *= radix


def head_pick(of, first, heads, every, start):
    out = of[first : first + heads, :]
    for k in range(heads, every, heads):
        out = jnp.where(start == k, of[first + k : first + k + heads, :], out)
    return out


def own_lanes(product, top, heads):
    return jnp.concatenate(
        [product[top + h : top + h + 1, h * DV : (h + 1) * DV] for h in range(heads)], axis=0
    )


def device_of(place):
    _, behind, flip, _, _ = place
    at = lax.axis_index("tp")
    groups = lax.axis_size("tp") // 2
    return lax.rem(at // 2 + groups - behind, groups) * 2 + (lax.rem(at, 2) ^ flip)


def push(stage, outs, places, sems):
    copies, column = [], 0
    for out in outs:
        width = out.shape[1]
        top = 0
        for place in places:
            device_rows, _, _, first, size = place
            row = pl.multiple_of(device_of(place) * device_rows + first, 16)
            copies.append(
                pltpu.make_async_copy(
                    stage.at[top : top + size, column : column + width],
                    out.at[pl.ds(row, size), :],
                    sems.at[len(copies)],
                )
            )
            copies[-1].start()
            top += size
        column += width
    return copies


def rows_kernel(heads, places, kind, *refs):
    count = len(places)
    left_over = list(refs)

    def take(n=1):
        got = left_over[:n]
        del left_over[:n]
        return got

    x_refs = take(count)
    key_ref, value_ref, gate_ref, forget_ref, bias_ref, query_ref = take(6)
    (token_ref,) = take() if kind == "first" else (None,)
    earlier = list(zip(take(count), take(count), strict=True)) if kind in ("more", "last") else None
    others = list(zip(take(2), take(2), strict=True)) if kind == "last" else []
    if kind in ("next", "start", "more"):
        take(2)
    if kind == "last":
        stage, sent_ref, log_ref = take(3)
    else:
        caches = take(2)
        state_refs, weight_refs = take(count), take(count)
        (kept_ref,) = take() if kind == "first" else (None,)
        stage, sems = take(2)
    x_ref, left_ref = take(2)
    (slots,) = take() if kind == "last" else (None,)
    depth = key_ref.shape[0]
    every = gate_ref.shape[0]
    at = lax.axis_index("tp")
    start = at * heads
    tops, total = [], 0
    for ref in x_refs:
        tops.append(total)
        x_ref[total : total + ref.shape[0], :] = ref[...]
        total += ref.shape[0]
    if token_ref is not None:
        row = lax.broadcasted_iota(jnp.int32, (16, depth), 0)
        token = jnp.where(row == 0, token_ref[...].astype(F32), 0.0)
        x_ref[total : total + 16, :] = token.astype(BF16)
    keys = key_ref.shape[1]
    stage[:, :keys] = jnp.dot(x_ref[...], key_ref[...], preferred_element_type=F32).astype(BF16)
    owner = lax.broadcasted_iota(jnp.int32, (heads, keys), 1) // DQK
    head = lax.broadcasted_iota(jnp.int32, (heads, keys), 0)
    query = jnp.where(owner == head, query_ref[...].astype(F32), 0.0).astype(BF16)
    left_ref[0:every, :] = gate_ref[...]
    left_ref[every : 2 * every, :] = forget_ref[...]
    gates = nt_dot(left_ref[...], x_ref[...])
    scores = nt_dot(query, stage[:, :keys]) * (1.0 / math.sqrt(DQK))
    stage[:, keys:] = jnp.dot(x_ref[...], value_ref[...], preferred_element_type=F32).astype(BF16)
    if kind != "last":
        copies = push(stage, caches, places, sems)
    diagonal = lax.broadcasted_iota(jnp.int32, (every, every), 0) == lax.broadcasted_iota(
        jnp.int32, (every, every), 1
    )
    bias = jnp.sum(jnp.where(diagonal, bias_ref[...], 0.0), axis=1, keepdims=True)
    log_forgets = log_sigmoid(
        head_pick(gates, every, heads, every, start) + head_pick(bias, 0, heads, every, start)
    )
    input_gate = head_pick(gates, 0, heads, every, start)
    if kind == "first":
        kept_ref[:, DV:] = lane_pack(
            {
                NEW_GATE: input_gate[:, total : total + 1],
                NEW_FORGET: log_forgets[:, total : total + 1],
                NEW_SCORE: scores[:, total : total + 1],
            },
            heads,
        )
        new_value = stage[total : total + 16, keys:].astype(F32)
        kept_ref[:, :DV] = jnp.concatenate(
            [new_value[0:1, h * DV : (h + 1) * DV] for h in range(heads)], axis=0
        )
    log_forget, input_gate, scores = log_forgets[:, :total], input_gate[:, :total], scores[:, :total]

    def piece_of(axis):
        index = lax.broadcasted_iota(jnp.int32, (total, total), axis)
        return sum((index >= top).astype(jnp.int32) for top in tops[1:]) if count > 1 else 0 * index

    later = (piece_of(0) == piece_of(1)) & (
        lax.broadcasted_iota(jnp.int32, (total, total), 0)
        > lax.broadcasted_iota(jnp.int32, (total, total), 1)
    )
    later = later.astype(F32).astype(BF16)
    high = log_forget.astype(BF16)
    rest = log_forget - high.astype(F32)
    middle = rest.astype(BF16)
    low = (rest - middle.astype(F32)).astype(BF16)

    def after(v):
        return jnp.dot(v, later, preferred_element_type=F32)

    log_weight = input_gate + (after(high) + (after(middle) + after(low)))
    lane = lax.broadcasted_iota(jnp.int32, (heads, total), 1)
    within = [
        (lane >= top) & (lane < top + ref.shape[0]) for top, ref in zip(tops, x_refs, strict=True)
    ]
    floor = jnp.finfo(jnp.float32).min
    peaks = [
        jnp.max(jnp.where(m, log_weight, floor), axis=1, keepdims=True) for m in within
    ]
    totals = [jnp.sum(jnp.where(m, log_forget, 0.0), axis=1, keepdims=True) for m in within]
    peak = jnp.zeros((heads, total), F32)
    for mask, value in zip(within, peaks, strict=True):
        peak = jnp.where(mask, value, peak)
    weighted = jnp.exp(log_weight - peak) * scores
    parts = [jnp.where(m, weighted, 0.0) for m in within]
    denoms = [jnp.sum(p, axis=1, keepdims=True) for p in parts]
    product = jnp.dot(
        jnp.concatenate(parts, axis=0).astype(BF16),
        stage[0:total, keys:],
        preferred_element_type=F32,
    )
    blocks = []
    for n, (top, place) in enumerate(zip(tops, places, strict=True)):
        _, _, _, first, size = place
        numer = own_lanes(product, n * heads, heads)
        mine = log_weight[:, top : top + size]
        now = (numer, totals[n], peaks[n], denoms[n])
        if earlier is not None:
            state_ref, weight_ref = earlier[n]
            stats = state_ref[:, DV:]
            before_peak = column(stats, PEAK) + totals[n]
            both = jnp.maximum(before_peak, peaks[n])
            was, new = jnp.exp(before_peak - both), jnp.exp(peaks[n] - both)
            now = (
                was * state_ref[:, :DV] + new * numer,
                column(stats, TOTAL) + totals[n],
                both,
                was * column(stats, DENOM) + new * denoms[n],
            )
            mine = jnp.concatenate([weight_ref[:, :first] + totals[n], mine], axis=1)
        blocks.append((device_of(place), now, mine))
    if kind != "last":
        for (_, now, mine), state_ref, weight_ref in zip(
            blocks, state_refs, weight_refs, strict=True
        ):
            numer, whole, top, denom = now
            state_ref[:, :DV] = numer
            state_ref[:, DV:] = lane_pack({TOTAL: whole, PEAK: top, DENOM: denom}, heads)
            weight_ref[...] = mine
        for copy in copies:
            copy.wait()
        return
    core = lax.rem(at, 2)
    for n, (state_ref, weight_ref) in enumerate(others):
        stats = state_ref[:, DV:]
        now = (state_ref[:, :DV], *(column(stats, k) for k in (TOTAL, PEAK, DENOM)))
        blocks.append((at if n == 0 else at - core + (1 - core), now, weight_ref[...]))
    for device, (numer, whole, top, denom), _ in blocks:
        slots[device, :, :DV] = numer
        slots[device, :, DV:] = lane_pack({TOTAL: whole, PEAK: top, DENOM: denom}, heads)
    devices = slots.shape[0]
    carry, _ = carries([slots[k, :, DV + TOTAL : DV + TOTAL + 1] for k in range(devices)])
    numer, denom, whole, top, _ = merge(slots, 0, heads)
    sent_ref[:, :DV] = numer
    sent_ref[:, DV:] = lane_pack(
        {TOTAL: whole, PEAK: top, DENOM: denom, CARRIED: jnp.zeros_like(whole)}, heads
    )
    for device, _, mine in blocks:
        carried = jnp.zeros((heads, 1), F32)
        for k in range(devices):
            carried = carried + jnp.where(device == k, carry[k], 0.0)
        length = mine.shape[1]
        log_ref[:, pl.ds(pl.multiple_of(device * length, length), length)] = mine + carried


def rows_call(kind, pieces, common, heads, token=None, earlier=(), others=(), caches=None):
    key_weight, value_weight = common[:2]
    depth, keys = key_weight.shape
    values = value_weight.shape[1]
    xs = [x for x, _ in pieces]
    places = tuple(p for _, p in pieces)
    device_rows = places[0][0]
    devices = lax.axis_size("tp")
    total = sum(x.shape[0] for x in xs) + (16 if kind == "first" else 0)
    hbm = pl.BlockSpec(memory_space=pl.ANY)
    args = [*xs, *common]
    if kind == "first":
        args.append(token)
    args += [s for s, _ in earlier] + [w for _, w in earlier]
    args += [s for s, _ in others] + [w for _, w in others]
    in_specs = [vmem()] * len(args)
    aliases = {}
    if kind in ("next", "start", "more"):
        aliases = {len(args): 0, len(args) + 1: 1}
        args += list(caches)
        in_specs += [hbm, hbm]
    state = jax.ShapeDtypeStruct((heads, DV + LANES), F32)
    scratch = [
        pltpu.VMEM((total, depth), BF16),
        pltpu.VMEM((2 * common[2].shape[0], depth), BF16),
    ]
    if kind == "last":
        outs = [
            jax.ShapeDtypeStruct((total, keys + values), BF16),
            state,
            jax.ShapeDtypeStruct((heads, devices * device_rows), F32),
        ]
        out_specs = [vmem()] * 3
        scratch.append(pltpu.VMEM((devices, heads, DV + LANES), F32))
    else:
        outs = [
            jax.ShapeDtypeStruct((devices * device_rows, keys), BF16),
            jax.ShapeDtypeStruct((devices * device_rows, values), BF16),
        ]
        outs += [state] * len(xs)
        outs += [jax.ShapeDtypeStruct((heads, p[3] + p[4]), F32) for p in places]
        outs += [state] if kind == "first" else []
        out_specs = [hbm, hbm] + [vmem()] * (len(outs) - 2)
        scratch = [
            pltpu.VMEM((total, keys + values), BF16),
            pltpu.SemaphoreType.DMA((2 * len(xs),)),
            *scratch,
        ]
    return pl.pallas_call(
        functools.partial(rows_kernel, heads, places, kind),
        out_shape=tuple(outs),
        in_specs=in_specs,
        out_specs=tuple(out_specs),
        scratch_shapes=scratch,
        input_output_aliases=aliases,
        compiler_params=params(),
        cost_estimate=cost(2 * total * depth * (keys + values), 2 * depth * (keys + values)),
        name="rows",
    )(*args)


def flush_kernel(places, stage, *refs):
    *outs, sems = refs[2:]
    for copy in push(stage, outs, places, sems):
        copy.wait()


def flush(stage, places, caches):
    hbm = pl.BlockSpec(memory_space=pl.ANY)
    return pl.pallas_call(
        functools.partial(flush_kernel, places),
        out_shape=tuple(jax.ShapeDtypeStruct(c.shape, c.dtype) for c in caches),
        in_specs=[vmem(), hbm, hbm],
        out_specs=(hbm, hbm),
        scratch_shapes=[pltpu.SemaphoreType.DMA((2 * len(places),))],
        input_output_aliases={1: 0, 2: 1},
        compiler_params=params(4),
        cost_estimate=cost(1e6, 1e6),
        name="flush",
    )(stage, *caches)


def body(
    prompt_tokens,
    key_weight,
    value_weight,
    input_weight,
    forget_weight,
    forget_bias,
    new_token,
    new_query,
):
    rows, _ = prompt_tokens.shape
    heads = key_weight.shape[1] // DQK
    devices = lax.axis_size("tp")
    chips = devices // 2
    first, spans = 0, []
    for share in (2, 4, 4):
        spans.append((first, rows // share))
        first += rows // share

    def to_core(v):
        return lax.ppermute(v, "tp", [(i, i ^ 1) for i in range(devices)])

    def to_chip(v, ahead):
        return lax.ppermute(
            v,
            "tp",
            [(i, ((i // 2 + ahead) % chips) * 2 + i % 2) for i in range(devices)],
        )

    ahead = range(1, chips)
    came = [[to_chip(prompt_tokens[a : a + size], d) for d in ahead] for a, size in spans]
    other = to_core(prompt_tokens)
    common = (
        key_weight,
        value_weight,
        input_weight.T,
        forget_weight.T,
        forget_bias.reshape(1, -1),
        new_query.reshape(1, -1),
    )

    def pieces(n):
        out = []
        for d, v in zip(ahead, came[n], strict=True):
            out.append((v, (rows, d, 0, *spans[n])))
            out.append((to_core(v), (rows, d, 1, *spans[n])))
        return out

    *caches, own_state, own_weight, kept = rows_call(
        "first",
        [(prompt_tokens, (rows, 0, 0, 0, rows))],
        common,
        heads,
        token=new_token.reshape(1, -1),
    )
    *caches, other_state, other_weight = rows_call(
        "next", [(other, (rows, 0, 1, 0, rows))], common, heads, caches=caches
    )
    states = ()
    for n in range(len(spans) - 1):
        those = pieces(n)
        out = rows_call(
            "more" if n else "start", those, common, heads, earlier=states, caches=caches
        )
        caches, out = out[:2], out[2:]
        states = tuple(zip(out[: len(those)], out[len(those) :], strict=True))
    those = pieces(len(spans) - 1)
    stage, sent, log_weight = rows_call(
        "last",
        those,
        common,
        heads,
        earlier=states,
        others=((own_state, own_weight), (other_state, other_weight)),
    )
    caches = flush(stage, tuple(p for _, p in those), caches)
    cache_weight, reading = exchange(sent, kept, log_weight, lax.axis_size("sp"))
    return (*caches, cache_weight, reading.reshape(-1))


def solution(mesh):
    placed = (P(("sp", "tp"), None), P(None, "tp"), P(None, "tp"), P(), P(), P(), P(), P("tp"))

    return jax.shard_map(
        body,
        mesh=mesh,
        in_specs=placed,
        out_specs=(P("sp", "tp"), P("sp", "tp"), P("tp", "sp"), P("tp")),
        check_vma=False,
    )
```

time: 139 us -> 56.1 us (0.40)
  blocking collectives: 57.8 us -> 0 us
  matrix products: 19.5 us -> 0 us
  Pallas kernels: 0 us -> 15.4 us
  local copies, waits for them, and re-layouts: 22.2 us -> 7.56 us
  between operations: 14.8 us -> 0.82 us
  starting transfers between devices: 0.04 us -> 11.5 us
  other arithmetic: 5.51 us -> 0 us
  waiting for transfers between devices: 18.1 us -> 20.6 us
    unnamed x1 -> x0, blocking collectives: 21.3 us -> none
    ppermute x0 -> x11, waiting for transfers between devices: none -> 20.6 us  [the longest x3 15.5 us: to_chip(): lax.ppermute(v, 'tp', [(i, (i // 2 + ahead) % chips * 2 + i % 2) for i in...]
    dot_general x7 -> x0, matrix products: 19.5 us -> none  [the longest x1 13.5 us: body(): jnp.dot(lax.all_gather(prompt_tokens, 'tp', axis=0, tiled=True), packed,...]
    psum x1 -> x0, blocking collectives: 19.4 us -> none  [body(): numerator, denominator = lax.psum((numer_part, denom_part), 'sp')]
    all_gather x1 -> x0, waiting for transfers between devices: 17.5 us -> none  [body(): lax.all_gather(prompt_tokens, 'tp', axis=0, tiled=True)]
    pmax x1 -> x0, blocking collectives: 17.1 us -> none  [body(): peak_log = lax.pmax(jnp.max(log_weight, axis=0), 'sp')]
    pallas_call x0 -> x8, Pallas kernels: none -> 15.4 us  [the longest x5 13.5 us: rows_call(): pl.pallas_call(functools.partial(rows_kernel, heads, places, kind), out_s...]
    ppermute x0 -> x11, starting transfers between devices: none -> 11.5 us  [the longest x4 6.23 us: to_stage(): return lax.ppermute(message, 'sp', [(i, i ^ flip) for i in range(peers)])]
  transfers between devices with their start and end apart: 1 -> 11, of which waited for: 1 -> 6; matrix products, arithmetic and copies ran while one was open for 15% -> 2% of each run, Pallas kernels for 0% -> 23%
where the time goes in v1:
time: 56.1 us; the launch traced here: 55.8 us
  waiting for transfers between devices  20.6 us (37%)
  Pallas kernels  15.4 us (27%)
  starting transfers between devices  11.5 us (20%)
  local copies, waits for them, and re-layouts  7.56 us (13%)
  between operations  0.82 us (1%)
    ppermute x3, waiting for transfers between devices, to_chip(): lax.ppermute(v, 'tp', [(i, (i // 2 + ahead) % chips * 2 + i % 2) for i in...  15.5 us
    pallas_call x5, Pallas kernels, rows_call(): pl.pallas_call(functools.partial(rows_kernel, heads, places, kind), out_s...  13.5 us
    ppermute x4, starting transfers between devices, to_stage(): return lax.ppermute(message, 'sp', [(i, i ^ flip) for i in range(peers)])  6.23 us
    unnamed x22, local copies, waits for them, and re-layouts  5.24 us
    ppermute x3, starting transfers between devices, to_chip(): lax.ppermute(v, 'tp', [(i, (i // 2 + ahead) % chips * 2 + i % 2) for i in...  5.15 us
    ppermute x4, waiting for transfers between devices, to_stage(): return lax.ppermute(message, 'sp', [(i, i ^ flip) for i in range(peers)])  5.06 us
    slice x2, local copies, waits for them, and re-layouts, body(): prompt_tokens[a:a + size]  2.3 us
  transfers between devices with their start and end apart: 11, of which 6 were waited for; matrix products, arithmetic and copies ran while one was open for 2% of the time, Pallas kernels for 23%

profile of v1, /device:TPU:0, one launch (start us, length us, event | category | flops | bytes accessed | tf_op | source)
XLA Modules:
  0.0 55.8 jit_solution(9866747548892053139)
XLA Ops:
  0.6 0.0 copy-start.10
  0.6 0.0 copy-start.9
  0.7 0.0 copy-start.8
  0.7 0.0 copy-start.2
  0.7 1.2 %slice.11 = bf16[128,2048]{1,0:T(8,128)(2,1)S(1)} slice(bf16[256,2048]{1,0:T(8,128)(2,1)} %refs_0_.1), slice={[0:128], [0:2048]} | slice | bytes 1048576 | tf_op jit(solution)/shard_map/slice | solution.py:478
  1.9 3.1 %collective-permute-start.4 = (bf16[128,2048]{1,0:T(8,128)(2,1)S(1)}, bf16[128,2048]{1,0:T(8,128)(2,1)S(1)}, u32[]{:S(2)}, u32[]{:S(2)}) collective-permute-start(bf16[128,2048]{1,0:T(8,128)(2,1)S(1)} %slice.11), channel_id=1, source_target_pairs={{0,2},{1,3},{2,0},{3,1},{4,6},{5,7},{6,4},{7,5},{8,10},{9,11},{10,... | collective-permute-start | bytes 1572872 | tf_op jit(solution)/shard_map/ppermute | solution.py:471
  5.0 0.0 collective-permute-start.6
  5.0 11.9 %collective-permute-done.4.refs_0_ = bf16[128,2048]{1,0:T(8,128)(2,1)S(1)} collective-permute-done((bf16[128,2048]{1,0:T(8,128)(2,1)S(1)}, bf16[128,2048]{1,0:T(8,128)(2,1)S(1)}, u32[]{:S(2)}, u32[]{:S(2)}) %collective-permute-start.4) | collective-permute-done | bytes 524320 | tf_op jit(solution)/shard_map/ppermute | solution.py:471
  16.9 0.0 collective-permute-start.5
  16.9 1.1 %fusion = (bf16[64,2048]{1,0:T(8,128)(2,1)S(1)}, bf16[64,2048]{1,0:T(8,128)(2,1)S(1)}) fusion(bf16[256,2048]{1,0:T(8,128)(2,1)} %refs_0_.1), kind=kLoop, calls=%fused_computation | loop fusion | bytes 1048576 | tf_op jit(solution)/shard_map/slice | solution.py:478
  18.0 1.8 %collective-permute-start.2 = (bf16[64,2048]{1,0:T(8,128)(2,1)S(1)}, bf16[64,2048]{1,0:T(8,128)(2,1)S(1)}, u32[]{:S(2)}, u32[]{:S(2)}) collective-permute-start(bf16[64,2048]{1,0:T(8,128)(2,1)S(1)} %get-tuple-element.60), channel_id=1, source_target_pairs={{0,2},{1,3},{2,0},{3,1},{4,6},{5,7},{6,4},{7,5},{8,10},{9,11},{10,... | collective-permute-start | bytes 786440 | tf_op jit(solution)/shard_map/ppermute | solution.py:471
  19.8 0.3 collective-permute-start
  20.1 0.0 copy-done.10
  20.1 0.0 copy-done.9
  20.1 0.0 copy-done.8
  20.1 0.0 copy-done.2
  20.1 0.0 copy-start
  20.1 2.2 %copy-done = bf16[2048,1024]{1,0:T(8,128)(2,1)S(1)} copy-done((bf16[2048,1024]{1,0:T(8,128)(2,1)S(1)}, bf16[2048,1024]{1,0:T(8,128)(2,1)}, u32[]{:S(2)}) %copy-start) | copy-done | bytes 4194328
  22.3 0.0 copy-start.3
  22.3 1.2 %copy-done.3 = bf16[256,2048]{1,0:T(8,128)(2,1)S(1)} copy-done((bf16[256,2048]{1,0:T(8,128)(2,1)S(1)}, bf16[256,2048]{1,0:T(8,128)(2,1)}, u32[]{:S(2)}) %copy-start.3) | copy-done | bytes 1048600
  23.5 0.0 copy-start.4
  23.5 0.9 %copy-done.4 = bf16[2048,32]{0,1:T(8,128)(2,1)S(1)} copy-done((bf16[2048,32]{0,1:T(8,128)(2,1)S(1)}, bf16[2048,32]{0,1:T(8,128)(2,1)}, u32[]{:S(2)}) %copy-start.4) | copy-done | bytes 131096
  24.4 0.0 copy-start.6
  24.4 0.9 %copy-done.6 = bf16[2048,32]{0,1:T(8,128)(2,1)S(1)} copy-done((bf16[2048,32]{0,1:T(8,128)(2,1)S(1)}, bf16[2048,32]{0,1:T(8,128)(2,1)}, u32[]{:S(2)}) %copy-start.6) | copy-done | bytes 131096
  25.3 0.0 copy-start.1
  25.3 0.0 copy-start.5
  25.3 0.0 copy-start.7
  25.3 3.4 %rows.5 = (bf16[1024,512]{1,0:T(8,128)(2,1)}, bf16[1024,1024]{1,0:T(8,128)(2,1)}, f32[8,256]{1,0:T(8,128)S(1)}, f32[8,256]{1,0:T(8,128)S(1)}, f32[8,256]{1,0:T(8,128)S(1)}) custom-call(bf16[256,2048]{1,0:T(8,128)(2,1)S(1)} %copy-done.3, bf16[2048,512]{1,0:T(8,128)(2,1)S(1)} %copy-done.2, bf16[2048,1024]{1,0:T(8,128)(2,1)S(1)} %copy-done, ...), custom_call_target="tpu_custom_call" | custom-call | flops 1711276032 | bytes 6291456 | tf_op jit(solution)/shard_map/rows/pallas_call | solution.py:414
  28.7 0.0 collective-permute-done.2.refs_0_
  28.7 0.1 collective-permute-start.3
  28.8 3.6 %collective-permute-done.refs_0_ = bf16[64,2048]{1,0:T(8,128)(2,1)S(1)} collective-permute-done((bf16[64,2048]{1,0:T(8,128)(2,1)S(1)}, bf16[64,2048]{1,0:T(8,128)(2,1)S(1)}, u32[]{:S(2)}, u32[]{:S(2)}) %collective-permute-start) | collective-permute-done | bytes 262176 | tf_op jit(solution)/shard_map/ppermute | solution.py:471
  32.4 0.0 collective-permute-start.1
  32.4 0.0 collective-permute-done.6.refs_0_
  32.4 0.0 copy-done.1
  32.4 0.0 copy-done.5
  32.4 0.0 copy-done.7
  32.4 3.2 %rows.6 = (bf16[1024,512]{1,0:T(8,128)(2,1)}, bf16[1024,1024]{1,0:T(8,128)(2,1)}, f32[8,256]{1,0:T(8,128)S(1)}, f32[8,256]{1,0:T(8,128)S(1)}) custom-call(bf16[256,2048]{1,0:T(8,128)(2,1)S(1)} %collective-permute-done.6.refs_0_, bf16[2048,512]{1,0:T(8,128)(2,1)S(1)} %copy-done.2, ...), custom_call_target="tpu_custom_call", output_to_operand_aliasing={{0}: (7, {}), {1}: (8, {})} | custom-call | flops 1610612736 | bytes 6291456 | tf_op jit(solution)/shard_map/rows/pallas_call | solution.py:414
  35.6 0.0 collective-permute-done.5.refs_1_
  35.6 3.2 %rows.7 = (bf16[1024,512]{1,0:T(8,128)(2,1)}, bf16[1024,1024]{1,0:T(8,128)(2,1)}, f32[8,256]{1,0:T(8,128)S(1)}, f32[8,256]{1,0:T(8,128)S(1)}, f32[8,128]{1,0:T(8,128)S(1)}, /*index=5*/f32[8,128]{1,0:T(8,128)S(1)}) custom-call(bf16[128,2048]{1,0:T(8,128)(2,1)S(1)} %collective-permute-done.4.refs_0_, ...), custom_call_target="tpu_custom_call", output_to_operand_aliasing={{0}: (8, {}), {1}: (9, {})} | custom-call | flops 1610612736 | bytes 6291456 | tf_op jit(solution)/shard_map/rows/pallas_call | solution.py:414
  38.8 0.0 collective-permute-done.3.refs_1_
  38.8 2.1 %rows.8 = (bf16[1024,512]{1,0:T(8,128)(2,1)}, bf16[1024,1024]{1,0:T(8,128)(2,1)}, f32[8,256]{1,0:T(8,128)S(1)}, f32[8,256]{1,0:T(8,128)S(1)}, f32[8,192]{1,0:T(8,128)S(1)}, /*index=5*/f32[8,192]{1,0:T(8,128)S(1)}) custom-call(bf16[64,2048]{1,0:T(8,128)(2,1)S(1)} %collective-permute-done.2.refs_0_, ...), custom_call_target="tpu_custom_call", output_to_operand_aliasing={{0}: (12, {}), {1}: (13, {})} | custom-call | flops 805306368 | bytes 6291456 | tf_op jit(solution)/shard_map/rows/pallas_call | solution.py:414
  40.9 0.0 collective-permute-done.1.refs_1_
  41.0 1.7 %rows.9 = (bf16[128,1536]{1,0:T(8,128)(2,1)S(1)}, f32[8,256]{1,0:T(8,128)S(1)}, f32[8,1024]{1,0:T(8,128)S(1)}) custom-call(bf16[64,2048]{1,0:T(8,128)(2,1)S(1)} %collective-permute-done.refs_0_, bf16[64,2048]{1,0:T(8,128)(2,1)S(1)} %collective-permute-done.1.refs_1_, bf16[2048,512]{1,0:T(8,128)(2,1)S(1)} %copy-done.2, bf16[2048,1024]{1,0:T(8,128)(2,1)S(1)} %copy-done.1, ...), custom_call_target="tpu_custom_call" | custom-call | flops 805306368 | bytes 6291456 | tf_op jit(solution)/shard_map/rows/pallas_call | solution.py:414
  42.6 1.8 %collective-permute-start.7 = (f32[8,256]{1,0:T(8,128)S(1)}, f32[8,256]{1,0:T(8,128)S(1)}, u32[]{:S(2)}, u32[]{:S(2)}) collective-permute-start(f32[8,256]{1,0:T(8,128)S(1)} %get-tuple-element.55.refs_0_), channel_id=1, source_target_pairs={{0,4},{4,0},{8,12},{12,8},{16,20},{20,16},{24,28},{28,24},{1,5},{5... | collective-permute-start | bytes 24584 | tf_op jit(solution)/shard_map/ppermute | solution.py:119
  44.4 1.9 %collective-permute-done.7.refs_1_ = f32[8,256]{1,0:T(8,128)S(1)} collective-permute-done((f32[8,256]{1,0:T(8,128)S(1)}, f32[8,256]{1,0:T(8,128)S(1)}, u32[]{:S(2)}, u32[]{:S(2)}) %collective-permute-start.7) | collective-permute-done | bytes 8224 | tf_op jit(solution)/shard_map/ppermute | solution.py:119
  46.3 0.1 merge.1.refs_0_
  46.5 3.8 %collective-permute-start.10 = (f32[8,256]{1,0:T(8,128)S(1)}, f32[8,256]{1,0:T(8,128)S(1)}, u32[]{:S(2)}, u32[]{:S(2)}) collective-permute-start(f32[8,256]{1,0:T(8,128)S(1)} %merge.1.refs_0_), channel_id=1, source_target_pairs={{0,24},{4,28},{8,16},{12,20},{16,8},{20,12},{24,0},{28,4},{1,25},{... | collective-permute-start | bytes 24584 | tf_op jit(solution)/shard_map/ppermute | solution.py:119
  50.3 0.0 collective-permute-start.8
  50.3 0.6 %collective-permute-start.9 = (f32[8,256]{1,0:T(8,128)S(1)}, f32[8,256]{1,0:T(8,128)S(1)}, u32[]{:S(2)}, u32[]{:S(2)}) collective-permute-start(f32[8,256]{1,0:T(8,128)S(1)} %merge.1.refs_0_), channel_id=1, source_target_pairs={{0,16},{4,20},{8,24},{12,28},{16,0},{20,4},{24,8},{28,12},{1,17},{... | collective-permute-start | bytes 24584 | tf_op jit(solution)/shard_map/ppermute | solution.py:119
  51.0 0.8 %flush.1 = (bf16[1024,512]{1,0:T(8,128)(2,1)}, bf16[1024,1024]{1,0:T(8,128)(2,1)}) custom-call(bf16[128,1536]{1,0:T(8,128)(2,1)S(1)} %get-tuple-element.50.stage, bf16[1024,512]{1,0:T(8,128)(2,1)} %get-tuple-element.51.refs_0_, bf16[1024,1024]{1,0:T(8,128)(2,1)} %get-tuple-element.52.refs_1_), custom_call_target="tpu_custom_call", output_to_operand_aliasing={{0}: (1, {}), {1}: (2, {})} | custom-call | flops 1000000 | bytes 1000000 | tf_op jit(solution)/shard_map/flush/pallas_call | solution.py:435
  51.7 0.2 collective-permute-done.10.refs_3_
  51.9 2.0 %collective-permute-done.8.refs_1_ = f32[8,256]{1,0:T(8,128)S(1)} collective-permute-done((f32[8,256]{1,0:T(8,128)S(1)}, f32[8,256]{1,0:T(8,128)S(1)}, u32[]{:S(2)}, u32[]{:S(2)}) %collective-permute-start.8) | collective-permute-done | bytes 8224 | tf_op jit(solution)/shard_map/ppermute | solution.py:119
  54.0 0.9 %collective-permute-done.9.refs_2_ = f32[8,256]{1,0:T(8,128)S(1)} collective-permute-done((f32[8,256]{1,0:T(8,128)S(1)}, f32[8,256]{1,0:T(8,128)S(1)}, u32[]{:S(2)}, u32[]{:S(2)}) %collective-permute-start.9) | collective-permute-done | bytes 8224 | tf_op jit(solution)/shard_map/ppermute | solution.py:119
  54.9 1.0 %finish.1 = (f32[8,1024]{1,0:T(8,128)}, f32[8,128]{1,0:T(8,128)}) custom-call(f32[8,256]{1,0:T(8,128)S(1)} %merge.1.refs_0_, f32[8,256]{1,0:T(8,128)S(1)} %collective-permute-done.8.refs_1_, f32[8,256]{1,0:T(8,128)S(1)} %collective-permute-done.9.refs_2_, f32[8,256]{1,0:T(8,128)S(1)} %collective-permute-done.10.refs_3_, ...), custom_call_target="tpu_custom_call" | custom-call | flops 1000000 | bytes 100000 | tf_op jit(solution)/shard_map/finish/pallas_call | solution.py:144
  (2 shorter events, 0.0 us)
Async XLA Ops:
  0.6 19.4 %copy-start.10 = (bf16[512]{0:T(512)(128)(2,1)S(1)}, bf16[512]{0:T(512)(128)(2,1)}, u32[]{:S(2)}) copy-start(bf16[512]{0:T(512)(128)(2,1)} %param.15) | copy-start | bytes 3076
  0.6 19.4 %copy-start.9 = (bf16[2048]{0:T(1024)(128)(2,1)S(1)}, bf16[2048]{0:T(1024)(128)(2,1)}, u32[]{:S(2)}) copy-start(bf16[2048]{0:T(1024)(128)(2,1)} %param.14) | copy-start | bytes 12292
  0.7 19.4 %copy-start.8 = (f32[32]{0:T(128)S(1)}, f32[32]{0:T(128)}, u32[]{:S(2)}) copy-start(f32[32]{0:T(128)} %param.13) | copy-start | bytes 388
  0.7 19.4 %copy-start.2 = (bf16[2048,512]{1,0:T(8,128)(2,1)S(1)}, bf16[2048,512]{1,0:T(8,128)(2,1)}, u32[]{:S(2)}) copy-start(bf16[2048,512]{1,0:T(8,128)(2,1)} %refs_2_.9) | copy-start | bytes 6291460
  1.9 15.0 %collective-permute-start.4 = (bf16[128,2048]{1,0:T(8,128)(2,1)S(1)}, bf16[128,2048]{1,0:T(8,128)(2,1)S(1)}, u32[]{:S(2)}, u32[]{:S(2)}) collective-permute-start(bf16[128,2048]{1,0:T(8,128)(2,1)S(1)} %slice.11), channel_id=1, source_target_pairs={{0,2},{1,3},{2,0},{3,1},{4,6},{5,7},{6,4},{7,5},{8,10},{9,11},{10,... | collective-permute-start | bytes 1572872 | tf_op jit(solution)/shard_map/ppermute | solution.py:471
  5.0 27.4 %collective-permute-start.6 = (bf16[256,2048]{1,0:T(8,128)(2,1)}, bf16[256,2048]{1,0:T(8,128)(2,1)S(1)}, u32[]{:S(2)}, u32[]{:S(2)}) collective-permute-start(bf16[256,2048]{1,0:T(8,128)(2,1)} %refs_0_.1), channel_id=1, source_target_pairs={{0,1},{1,0},{2,3},{3,2},{4,5},{5,4},{6,7},{7,6},{8,9},{9,8},{10,11... | collective-permute-start | bytes 3145736 | tf_op jit(solution)/shard_map/ppermute | solution.py:468
  16.9 18.7 %collective-permute-start.5 = (bf16[128,2048]{1,0:T(8,128)(2,1)S(1)}, bf16[128,2048]{1,0:T(8,128)(2,1)S(1)}, u32[]{:S(2)}, u32[]{:S(2)}) collective-permute-start(bf16[128,2048]{1,0:T(8,128)(2,1)S(1)} %collective-permute-done.4.refs_0_), channel_id=1, source_target_pairs={{0,1},{1,0},{2,3},{3,2},{4,5},{5,4},{6,7},{7,6},{8,9},{9,8},{10,11... | collective-permute-start | bytes 1572872 | tf_op jit(solution)/shard_map/ppermute | solution.py:468
  18.0 10.7 %collective-permute-start.2 = (bf16[64,2048]{1,0:T(8,128)(2,1)S(1)}, bf16[64,2048]{1,0:T(8,128)(2,1)S(1)}, u32[]{:S(2)}, u32[]{:S(2)}) collective-permute-start(bf16[64,2048]{1,0:T(8,128)(2,1)S(1)} %get-tuple-element.60), channel_id=1, source_target_pairs={{0,2},{1,3},{2,0},{3,1},{4,6},{5,7},{6,4},{7,5},{8,10},{9,11},{10,... | collective-permute-start | bytes 786440 | tf_op jit(solution)/shard_map/ppermute | solution.py:471
  19.8 12.6 %collective-permute-start = (bf16[64,2048]{1,0:T(8,128)(2,1)S(1)}, bf16[64,2048]{1,0:T(8,128)(2,1)S(1)}, u32[]{:S(2)}, u32[]{:S(2)}) collective-permute-start(bf16[64,2048]{1,0:T(8,128)(2,1)S(1)} %get-tuple-element.61), channel_id=1, source_target_pairs={{0,2},{1,3},{2,0},{3,1},{4,6},{5,7},{6,4},{7,5},{8,10},{9,11},{10,... | collective-permute-start | bytes 786440 | tf_op jit(solution)/shard_map/ppermute | solution.py:471
  20.1 2.2 %copy-start = (bf16[2048,1024]{1,0:T(8,128)(2,1)S(1)}, bf16[2048,1024]{1,0:T(8,128)(2,1)}, u32[]{:S(2)}) copy-start(bf16[2048,1024]{1,0:T(8,128)(2,1)} %refs_3_.5) | copy-start | bytes 12582916
  22.3 1.2 %copy-start.3 = (bf16[256,2048]{1,0:T(8,128)(2,1)S(1)}, bf16[256,2048]{1,0:T(8,128)(2,1)}, u32[]{:S(2)}) copy-start(bf16[256,2048]{1,0:T(8,128)(2,1)} %refs_0_.1) | copy-start | bytes 3145732
  23.5 0.9 %copy-start.4 = (bf16[2048,32]{0,1:T(8,128)(2,1)S(1)}, bf16[2048,32]{0,1:T(8,128)(2,1)}, u32[]{:S(2)}) copy-start(bf16[2048,32]{0,1:T(8,128)(2,1)} %param.11) | copy-start | bytes 393220
  24.4 0.9 %copy-start.6 = (bf16[2048,32]{0,1:T(8,128)(2,1)S(1)}, bf16[2048,32]{0,1:T(8,128)(2,1)}, u32[]{:S(2)}) copy-start(bf16[2048,32]{0,1:T(8,128)(2,1)} %param.12) | copy-start | bytes 393220
  25.3 7.0 %copy-start.1 = (bf16[2048,1024]{1,0:T(8,128)(2,1)S(1)}, bf16[2048,1024]{1,0:T(8,128)(2,1)}, u32[]{:S(2)}) copy-start(bf16[2048,1024]{1,0:T(8,128)(2,1)} %refs_3_.5) | copy-start | bytes 12582916
  25.3 7.0 %copy-start.5 = (bf16[2048,32]{0,1:T(8,128)(2,1)S(1)}, bf16[2048,32]{0,1:T(8,128)(2,1)}, u32[]{:S(2)}) copy-start(bf16[2048,32]{0,1:T(8,128)(2,1)} %param.11) | copy-start | bytes 393220
  25.3 7.1 %copy-start.7 = (bf16[2048,32]{0,1:T(8,128)(2,1)S(1)}, bf16[2048,32]{0,1:T(8,128)(2,1)}, u32[]{:S(2)}) copy-start(bf16[2048,32]{0,1:T(8,128)(2,1)} %param.12) | copy-start | bytes 393220
  28.7 10.1 %collective-permute-start.3 = (bf16[64,2048]{1,0:T(8,128)(2,1)S(1)}, bf16[64,2048]{1,0:T(8,128)(2,1)S(1)}, u32[]{:S(2)}, u32[]{:S(2)}) collective-permute-start(bf16[64,2048]{1,0:T(8,128)(2,1)S(1)} %collective-permute-done.2.refs_0_), channel_id=1, source_target_pairs={{0,1},{1,0},{2,3},{3,2},{4,5},{5,4},{6,7},{7,6},{8,9},{9,8},{10,11... | collective-permute-start | bytes 786440 | tf_op jit(solution)/shard_map/ppermute | solution.py:468
  32.4 8.6 %collective-permute-start.1 = (bf16[64,2048]{1,0:T(8,128)(2,1)S(1)}, bf16[64,2048]{1,0:T(8,128)(2,1)S(1)}, u32[]{:S(2)}, u32[]{:S(2)}) collective-permute-start(bf16[64,2048]{1,0:T(8,128)(2,1)S(1)} %collective-permute-done.refs_0_), channel_id=1, source_target_pairs={{0,1},{1,0},{2,3},{3,2},{4,5},{5,4},{6,7},{7,6},{8,9},{9,8},{10,11... | collective-permute-start | bytes 786440 | tf_op jit(solution)/shard_map/ppermute | solution.py:468
  42.6 3.7 %collective-permute-start.7 = (f32[8,256]{1,0:T(8,128)S(1)}, f32[8,256]{1,0:T(8,128)S(1)}, u32[]{:S(2)}, u32[]{:S(2)}) collective-permute-start(f32[8,256]{1,0:T(8,128)S(1)} %get-tuple-element.55.refs_0_), channel_id=1, source_target_pairs={{0,4},{4,0},{8,12},{12,8},{16,20},{20,16},{24,28},{28,24},{1,5},{5... | collective-permute-start | bytes 24584 | tf_op jit(solution)/shard_map/ppermute | solution.py:119
  46.5 5.5 %collective-permute-start.10 = (f32[8,256]{1,0:T(8,128)S(1)}, f32[8,256]{1,0:T(8,128)S(1)}, u32[]{:S(2)}, u32[]{:S(2)}) collective-permute-start(f32[8,256]{1,0:T(8,128)S(1)} %merge.1.refs_0_), channel_id=1, source_target_pairs={{0,24},{4,28},{8,16},{12,20},{16,8},{20,12},{24,0},{28,4},{1,25},{... | collective-permute-start | bytes 24584 | tf_op jit(solution)/shard_map/ppermute | solution.py:119
  50.3 3.7 %collective-permute-start.8 = (f32[8,256]{1,0:T(8,128)S(1)}, f32[8,256]{1,0:T(8,128)S(1)}, u32[]{:S(2)}, u32[]{:S(2)}) collective-permute-start(f32[8,256]{1,0:T(8,128)S(1)} %merge.1.refs_0_), channel_id=1, source_target_pairs={{0,8},{4,12},{8,0},{12,4},{16,24},{20,28},{24,16},{28,20},{1,9},{5... | collective-permute-start | bytes 24584 | tf_op jit(solution)/shard_map/ppermute | solution.py:119
  50.3 4.5 %collective-permute-start.9 = (f32[8,256]{1,0:T(8,128)S(1)}, f32[8,256]{1,0:T(8,128)S(1)}, u32[]{:S(2)}, u32[]{:S(2)}) collective-permute-start(f32[8,256]{1,0:T(8,128)S(1)} %merge.1.refs_0_), channel_id=1, source_target_pairs={{0,16},{4,20},{8,24},{12,28},{16,0},{20,4},{24,8},{28,12},{1,17},{... | collective-permute-start | bytes 24584 | tf_op jit(solution)/shard_map/ppermute | solution.py:119

commit v2 on v1

--- a/solution.py
+++ b/solution.py
@@ -123,7 +123,7 @@
     heads, width = message.shape
     radices, left = [], peers
     while left > 1:
-        radices.append(4 if left % 4 == 0 and (left // 4 == 1 or radices) else 2)
+        radices.append(2 if left % 2 == 0 else left)
         left //= radices[-1]
     stride = 1
     for n, radix in enumerate(radices):
@@ -198,7 +198,7 @@
     return copies
 
 
-def rows_kernel(heads, places, kind, *refs):
+def rows_kernel(heads, places, arrays, kind, *refs):
     count = len(places)
     left_over = list(refs)
 
@@ -207,7 +207,7 @@
         del left_over[:n]
         return got
 
-    x_refs = take(count)
+    x_refs = take(arrays)
     key_ref, value_ref, gate_ref, forget_ref, bias_ref, query_ref = take(6)
     (token_ref,) = take() if kind == "first" else (None,)
     earlier = list(zip(take(count), take(count), strict=True)) if kind in ("more", "last") else None
@@ -227,9 +227,9 @@
     every = gate_ref.shape[0]
     at = lax.axis_index("tp")
     start = at * heads
-    tops, total = [], 0
+    tops = [sum(p[4] for p in places[:n]) for n in range(count)]
+    total = 0
     for ref in x_refs:
-        tops.append(total)
         x_ref[total : total + ref.shape[0], :] = ref[...]
         total += ref.shape[0]
     if token_ref is not None:
@@ -291,7 +291,7 @@
     log_weight = input_gate + (after(high) + (after(middle) + after(low)))
     lane = lax.broadcasted_iota(jnp.int32, (heads, total), 1)
     within = [
-        (lane >= top) & (lane < top + ref.shape[0]) for top, ref in zip(tops, x_refs, strict=True)
+        (lane >= top) & (lane < top + place[4]) for top, place in zip(tops, places, strict=True)
     ]
     floor = jnp.finfo(jnp.float32).min
     peaks = [
@@ -367,7 +367,7 @@
     key_weight, value_weight = common[:2]
     depth, keys = key_weight.shape
     values = value_weight.shape[1]
-    xs = [x for x, _ in pieces]
+    xs = [x for those, _ in pieces for x in those]
     places = tuple(p for _, p in pieces)
     device_rows = places[0][0]
     devices = lax.axis_size("tp")
@@ -402,17 +402,17 @@
             jax.ShapeDtypeStruct((devices * device_rows, keys), BF16),
             jax.ShapeDtypeStruct((devices * device_rows, values), BF16),
         ]
-        outs += [state] * len(xs)
+        outs += [state] * len(places)
         outs += [jax.ShapeDtypeStruct((heads, p[3] + p[4]), F32) for p in places]
         outs += [state] if kind == "first" else []
         out_specs = [hbm, hbm] + [vmem()] * (len(outs) - 2)
         scratch = [
             pltpu.VMEM((total, keys + values), BF16),
-            pltpu.SemaphoreType.DMA((2 * len(xs),)),
+            pltpu.SemaphoreType.DMA((2 * len(places),)),
             *scratch,
         ]
     return pl.pallas_call(
-        functools.partial(rows_kernel, heads, places, kind),
+        functools.partial(rows_kernel, heads, places, len(xs), kind),
         out_shape=tuple(outs),
         in_specs=in_specs,
         out_specs=tuple(out_specs),
@@ -422,6 +422,31 @@
         cost_estimate=cost(2 * total * depth * (keys + values), 2 * depth * (keys + values)),
         name="rows",
     )(*args)
+
+
+def cut_kernel(spans, x_ref, *refs):
+    *outs, sems = refs
+    copies = [
+        pltpu.make_async_copy(x_ref.at[pl.ds(first, size)], out, sems.at[n])
+        for n, ((first, size), out) in enumerate(zip(spans, outs, strict=True))
+    ]
+    for copy in copies:
+        copy.start()
+    for copy in copies:
+        copy.wait()
+
+
+def cut(x, spans):
+    return pl.pallas_call(
+        functools.partial(cut_kernel, spans),
+        out_shape=tuple(jax.ShapeDtypeStruct((size, x.shape[1]), x.dtype) for _, size in spans),
+        in_specs=[pl.BlockSpec(memory_space=pl.ANY)],
+        out_specs=tuple([vmem()] * len(spans)),
+        scratch_shapes=[pltpu.SemaphoreType.DMA((len(spans),))],
+        compiler_params=params(4),
+        cost_estimate=cost(8e9, 1e6),
+        name="cut",
+    )(x)
 
 
 def flush_kernel(places, stage, *refs):
@@ -443,6 +468,10 @@
         cost_estimate=cost(1e6, 1e6),
         name="flush",
     )(stage, *caches)
+
+
+UNITS = (4, 4, 4, 3, 1)
+TOGETHER = ((0, 1), (2,), (3, 4))
 
 
 def body(
@@ -459,23 +488,27 @@
     heads = key_weight.shape[1] // DQK
     devices = lax.axis_size("tp")
     chips = devices // 2
-    first, spans = 0, []
-    for share in (2, 4, 4):
-        spans.append((first, rows // share))
-        first += rows // share
+    unit, first, spans = rows // 16, 0, []
+    for units in UNITS:
+        spans.append((first, units * unit))
+        first += units * unit
+    blocks = [(spans[w[0]][0], sum(spans[n][1] for n in w)) for w in TOGETHER]
+    last = len(spans) - 1
 
     def to_core(v):
         return lax.ppermute(v, "tp", [(i, i ^ 1) for i in range(devices)])
 
-    def to_chip(v, ahead):
+    def to_chip(v, ahead, flip=0):
         return lax.ppermute(
             v,
             "tp",
-            [(i, ((i // 2 + ahead) % chips) * 2 + i % 2) for i in range(devices)],
+            [(i, (((i // 2 + ahead) % chips) * 2 + i % 2) ^ flip) for i in range(devices)],
         )
 
     ahead = range(1, chips)
-    came = [[to_chip(prompt_tokens[a : a + size], d) for d in ahead] for a, size in spans]
+    chunks = [prompt_tokens[: spans[0][1]], *cut(prompt_tokens, spans[1:])]
+    came = [[to_chip(v, d) for d in ahead] for v in chunks]
+    crossed = [to_chip(chunks[-1], d, 1) for d in ahead]
     other = to_core(prompt_tokens)
     common = (
         key_weight,
@@ -486,32 +519,34 @@
         new_query.reshape(1, -1),
     )
 
-    def pieces(n):
+    def pieces(which, block):
         out = []
-        for d, v in zip(ahead, came[n], strict=True):
-            out.append((v, (rows, d, 0, *spans[n])))
-            out.append((to_core(v), (rows, d, 1, *spans[n])))
+        for d in ahead:
+            straight = [came[n][d - 1] for n in which]
+            turned = [crossed[d - 1] if n == last else to_core(came[n][d - 1]) for n in which]
+            out.append((straight, (rows, d, 0, *block)))
+            out.append((turned, (rows, d, 1, *block)))
         return out
 
     *caches, own_state, own_weight, kept = rows_call(
         "first",
-        [(prompt_tokens, (rows, 0, 0, 0, rows))],
+        [(chunks, (rows, 0, 0, 0, rows))],
         common,
         heads,
         token=new_token.reshape(1, -1),
     )
     *caches, other_state, other_weight = rows_call(
-        "next", [(other, (rows, 0, 1, 0, rows))], common, heads, caches=caches
+        "next", [([other], (rows, 0, 1, 0, rows))], common, heads, caches=caches
     )
     states = ()
-    for n in range(len(spans) - 1):
-        those = pieces(n)
+    for n, which in enumerate(TOGETHER[:-1]):
+        those = pieces(which, blocks[n])
         out = rows_call(
             "more" if n else "start", those, common, heads, earlier=states, caches=caches
         )
         caches, out = out[:2], out[2:]
         states = tuple(zip(out[: len(those)], out[len(those) :], strict=True))
-    those = pieces(len(spans) - 1)
+    those = pieces(TOGETHER[-1], blocks[-1])
     stage, sent, log_weight = rows_call(
         "last",
         those,

time: 56.1 us -> 50.8 us (0.906)
  local copies, waits for them, and re-layouts: 7.56 us -> 1.62 us
  waiting for transfers between devices: 20.6 us -> 17.5 us
  starting transfers between devices: 11.5 us -> 14.6 us
  Pallas kernels: 15.4 us -> 16 us
    unnamed x22 -> x16, local copies, waits for them, and re-layouts: 5.24 us -> 1.59 us
    ppermute x3 -> x6, waiting for transfers between devices: 15.5 us -> 12.1 us  [to_chip(): lax.ppermute(v, 'tp', [(i, (i // 2 + ahead) % chips * 2 + i % 2 ^ flip) f...]
    slice x2 -> x1, local copies, waits for them, and re-layouts: 2.3 us -> 0.02 us  [body(): chunks = [prompt_tokens[:spans[0][1]], *cut(prompt_tokens, spans[1:])]]
    ppermute x3 -> x6, starting transfers between devices: 5.15 us -> 7.02 us  [to_chip(): lax.ppermute(v, 'tp', [(i, (i // 2 + ahead) % chips * 2 + i % 2 ^ flip) f...]
    ppermute x4 -> x5, starting transfers between devices: 0.09 us -> 1.91 us  [to_core(): return lax.ppermute(v, 'tp', [(i, i ^ 1) for i in range(devices)])]
    ppermute x4 -> x3, starting transfers between devices: 6.23 us -> 5.72 us  [to_stage(): return lax.ppermute(message, 'sp', [(i, i ^ flip) for i in range(peers)])]
    pallas_call x5 -> x6, Pallas kernels: 13.5 us -> 14 us  [the longest x5 13.6 us: rows_call(): pl.pallas_call(functools.partial(rows_kernel, heads, places, len(xs), kin...]
    ppermute x4 -> x3, waiting for transfers between devices: 5.06 us -> 5.4 us  [to_stage(): return lax.ppermute(message, 'sp', [(i, i ^ flip) for i in range(peers)])]
  transfers between devices with their start and end apart: 11 -> 14, of which waited for: 6 -> 6; matrix products, arithmetic and copies ran while one was open for 2% -> 0% of each run, Pallas kernels for 23% -> 26%
where the time goes in v2:
time: 50.8 us; the launch traced here: 50.6 us
  waiting for transfers between devices  17.5 us (34%)
  Pallas kernels  16 us (31%)
  starting transfers between devices  14.6 us (29%)
  local copies, waits for them, and re-layouts  1.62 us (3%)
  between operations  0.8 us (2%)
    pallas_call x5, Pallas kernels, rows_call(): pl.pallas_call(functools.partial(rows_kernel, heads, places, len(xs), kin...  13.6 us
    ppermute x6, waiting for transfers between devices, to_chip(): lax.ppermute(v, 'tp', [(i, (i // 2 + ahead) % chips * 2 + i % 2 ^ flip) f...  12.1 us
    ppermute x6, starting transfers between devices, to_chip(): lax.ppermute(v, 'tp', [(i, (i // 2 + ahead) % chips * 2 + i % 2 ^ flip) f...  7.02 us
    ppermute x3, starting transfers between devices, to_stage(): return lax.ppermute(message, 'sp', [(i, i ^ flip) for i in range(peers)])  5.72 us
    ppermute x3, waiting for transfers between devices, to_stage(): return lax.ppermute(message, 'sp', [(i, i ^ flip) for i in range(peers)])  5.4 us
    ppermute x5, starting transfers between devices, to_core(): return lax.ppermute(v, 'tp', [(i, i ^ 1) for i in range(devices)])  1.91 us
    unnamed x16, local copies, waits for them, and re-layouts  1.59 us
  transfers between devices with their start and end apart: 14, of which 6 were waited for; matrix products, arithmetic and copies ran while one was open for 0% of the time, Pallas kernels for 26%

profile of v2, /device:TPU:0, one launch (start us, length us, event | category | flops | bytes accessed | tf_op | source)
XLA Modules:
  0.0 50.6 jit_solution(9455355367590877662)
XLA Ops:
  0.6 0.0 copy-start.2
  0.6 0.0 copy-start.3
  0.7 0.0 copy-start
  0.7 0.0 copy-start.1
  0.7 0.6 %collective-permute-start.10 = (bf16[256,2048]{1,0:T(8,128)(2,1)}, bf16[256,2048]{1,0:T(8,128)(2,1)S(1)}, u32[]{:S(2)}, u32[]{:S(2)}) collective-permute-start(bf16[256,2048]{1,0:T(8,128)(2,1)} %x_ref.1), channel_id=1, source_target_pairs={{0,1},{1,0},{2,3},{3,2},{4,5},{5,4},{6,7},{7,6},{8,9},{9,8},{10,11... | collective-permute-start | bytes 3145736 | tf_op jit(solution)/shard_map/ppermute | solution.py:499
  1.2 0.0 copy-start.4
  1.2 1.6 %copy-done.4 = bf16[256,2048]{1,0:T(8,128)(2,1)S(1)} copy-done((bf16[256,2048]{1,0:T(8,128)(2,1)S(1)}, bf16[256,2048]{1,0:T(8,128)(2,1)}, u32[]{:S(2)}) %copy-start.4) | copy-done | bytes 1048600
  2.8 0.0 copy-start.7
  2.8 0.0 copy-start.6
  2.8 0.0 copy-start.5
  2.8 0.4 cut.1
  3.2 2.4 %collective-permute-start.7 = (bf16[64,2048]{1,0:T(8,128)(2,1)S(1)}, bf16[64,2048]{1,0:T(8,128)(2,1)S(1)}, u32[]{:S(2)}, u32[]{:S(2)}) collective-permute-start(bf16[64,2048]{1,0:T(8,128)(2,1)S(1)} %get-tuple-element.39.refs_1_), channel_id=1, source_target_pairs={{0,2},{1,3},{2,0},{3,1},{4,6},{5,7},{6,4},{7,5},{8,10},{9,11},{10,... | collective-permute-start | bytes 786440 | tf_op jit(solution)/shard_map/ppermute | solution.py:502
  5.6 0.1 collective-permute-start.6
  5.7 2.0 %collective-permute-start.4 = (bf16[64,2048]{1,0:T(8,128)(2,1)S(1)}, bf16[64,2048]{1,0:T(8,128)(2,1)S(1)}, u32[]{:S(2)}, u32[]{:S(2)}) collective-permute-start(bf16[64,2048]{1,0:T(8,128)(2,1)S(1)} %get-tuple-element.38.refs_2_), channel_id=1, source_target_pairs={{0,2},{1,3},{2,0},{3,1},{4,6},{5,7},{6,4},{7,5},{8,10},{9,11},{10,... | collective-permute-start | bytes 786440 | tf_op jit(solution)/shard_map/ppermute | solution.py:502
  7.7 0.1 collective-permute-start
  7.8 0.0 copy-done.7
  7.8 0.0 copy-done.6
  7.8 4.9 %collective-permute-done.7.refs_1_ = bf16[64,2048]{1,0:T(8,128)(2,1)S(1)} collective-permute-done((bf16[64,2048]{1,0:T(8,128)(2,1)S(1)}, bf16[64,2048]{1,0:T(8,128)(2,1)S(1)}, u32[]{:S(2)}, u32[]{:S(2)}) %collective-permute-start.7) | collective-permute-done | bytes 262176 | tf_op jit(solution)/shard_map/ppermute | solution.py:502
  12.7 0.3 collective-permute-start.9
  13.0 5.3 %collective-permute-done.6.refs_0_ = bf16[64,2048]{1,0:T(8,128)(2,1)S(1)} collective-permute-done((bf16[64,2048]{1,0:T(8,128)(2,1)S(1)}, bf16[64,2048]{1,0:T(8,128)(2,1)S(1)}, u32[]{:S(2)}, u32[]{:S(2)}) %collective-permute-start.6) | collective-permute-done | bytes 262176 | tf_op jit(solution)/shard_map/ppermute | solution.py:502
  18.3 0.3 collective-permute-start.8
  18.6 0.0 copy-done.2
  18.6 0.0 copy-done.3
  18.6 0.0 copy-done
  18.6 0.0 copy-done.1
  18.6 0.0 copy-done.5
  18.6 3.4 %rows.5 = (bf16[1024,512]{1,0:T(8,128)(2,1)}, bf16[1024,1024]{1,0:T(8,128)(2,1)}, f32[8,256]{1,0:T(8,128)S(1)}, f32[8,256]{1,0:T(8,128)S(1)}, f32[8,256]{1,0:T(8,128)S(1)}) custom-call(bf16[64,2048]{1,0:T(8,128)(2,1)S(1)} %slice.3.refs_0_, bf16[64,2048]{1,0:T(8,128)(2,1)S(1)} %get-tuple-element.39.refs_1_, bf16[64,2048]{1,0:T(8,128)(2,1)S(1)} %get-tuple-element.38.refs_2_, ...), custom_call_target="tpu_custom_call" | custom-call | flops 1711276032 | bytes 6291456 | tf_op jit(solution)/shard_map/rows/pallas_call | solution.py:414
  22.0 1.9 %collective-permute-done.4.refs_0_ = bf16[64,2048]{1,0:T(8,128)(2,1)S(1)} collective-permute-done((bf16[64,2048]{1,0:T(8,128)(2,1)S(1)}, bf16[64,2048]{1,0:T(8,128)(2,1)S(1)}, u32[]{:S(2)}, u32[]{:S(2)}) %collective-permute-start.4) | collective-permute-done | bytes 262176 | tf_op jit(solution)/shard_map/ppermute | solution.py:502
  23.9 2.1 %collective-permute-start.1 = (bf16[16,2048]{1,0:T(8,128)(2,1)S(1)}, bf16[16,2048]{1,0:T(8,128)(2,1)S(1)}, u32[]{:S(2)}, u32[]{:S(2)}) collective-permute-start(bf16[16,2048]{1,0:T(8,128)(2,1)S(1)} %get-tuple-element.37.refs_4_), channel_id=1, source_target_pairs={{0,2},{1,3},{2,0},{3,1},{4,6},{5,7},{6,4},{7,5},{8,10},{9,11},{10,... | collective-permute-start | bytes 196616 | tf_op jit(solution)/shard_map/ppermute | solution.py:502
  26.0 0.0 collective-permute-done.10.refs_0_
  26.0 0.0 collective-permute-start.5
  26.0 3.2 %rows.6 = (bf16[1024,512]{1,0:T(8,128)(2,1)}, bf16[1024,1024]{1,0:T(8,128)(2,1)}, f32[8,256]{1,0:T(8,128)S(1)}, f32[8,256]{1,0:T(8,128)S(1)}) custom-call(bf16[256,2048]{1,0:T(8,128)(2,1)S(1)} %collective-permute-done.10.refs_0_, bf16[2048,512]{1,0:T(8,128)(2,1)S(1)} %copy-done.1, ...), custom_call_target="tpu_custom_call", output_to_operand_aliasing={{0}: (7, {}), {1}: (8, {})} | custom-call | flops 1610612736 | bytes 6291456 | tf_op jit(solution)/shard_map/rows/pallas_call | solution.py:414
  29.2 0.0 collective-permute-done.refs_0_
  29.2 0.3 collective-permute-start.3
  29.6 0.0 collective-permute-done.9.refs_3_
  29.6 0.8 %collective-permute-start.2 = (bf16[48,2048]{1,0:T(8,128)(2,1)S(1)}, bf16[48,2048]{1,0:T(8,128)(2,1)S(1)}, u32[]{:S(2)}, u32[]{:S(2)}) collective-permute-start(bf16[48,2048]{1,0:T(8,128)(2,1)S(1)} %collective-permute-done.refs_0_), channel_id=1, source_target_pairs={{0,1},{1,0},{2,3},{3,2},{4,5},{5,4},{6,7},{7,6},{8,9},{9,8},{10,11... | collective-permute-start | bytes 589832 | tf_op jit(solution)/shard_map/ppermute | solution.py:499
  30.4 0.0 collective-permute-done.8.refs_2_
  30.4 3.2 %rows.7 = (bf16[1024,512]{1,0:T(8,128)(2,1)}, bf16[1024,1024]{1,0:T(8,128)(2,1)}, f32[8,256]{1,0:T(8,128)S(1)}, f32[8,256]{1,0:T(8,128)S(1)}, f32[8,128]{1,0:T(8,128)S(1)}, /*index=5*/f32[8,128]{1,0:T(8,128)S(1)}) custom-call(bf16[64,2048]{1,0:T(8,128)(2,1)S(1)} %collective-permute-done.6.refs_0_, ...), custom_call_target="tpu_custom_call", output_to_operand_aliasing={{0}: (10, {}), {1}: (11, {})} | custom-call | flops 1610612736 | bytes 6291456 | tf_op jit(solution)/shard_map/rows/pallas_call | solution.py:414
  33.5 0.0 collective-permute-done.5.refs_1_
  33.6 2.1 %rows.8 = (bf16[1024,512]{1,0:T(8,128)(2,1)}, bf16[1024,1024]{1,0:T(8,128)(2,1)}, f32[8,256]{1,0:T(8,128)S(1)}, f32[8,256]{1,0:T(8,128)S(1)}, f32[8,192]{1,0:T(8,128)S(1)}, /*index=5*/f32[8,192]{1,0:T(8,128)S(1)}) custom-call(bf16[64,2048]{1,0:T(8,128)(2,1)S(1)} %collective-permute-done.4.refs_0_, ...), custom_call_target="tpu_custom_call", output_to_operand_aliasing={{0}: (12, {}), {1}: (13, {})} | custom-call | flops 805306368 | bytes 6291456 | tf_op jit(solution)/shard_map/rows/pallas_call | solution.py:414
  35.7 0.0 collective-permute-done.1.refs_1_
  35.7 0.0 collective-permute-done.3.refs_3_
  35.7 0.0 collective-permute-done.2.refs_2_
  35.7 1.7 %rows.9 = (bf16[128,1536]{1,0:T(8,128)(2,1)S(1)}, f32[8,256]{1,0:T(8,128)S(1)}, f32[8,1024]{1,0:T(8,128)S(1)}) custom-call(bf16[48,2048]{1,0:T(8,128)(2,1)S(1)} %collective-permute-done.refs_0_, bf16[16,2048]{1,0:T(8,128)(2,1)S(1)} %collective-permute-done.1.refs_1_, bf16[48,2048]{1,0:T(8,128)(2,1)S(1)} %collective-permute-done.2.refs_2_, ...), custom_call_target="tpu_custom_call" | custom-call | flops 805306368 | bytes 6291456 | tf_op jit(solution)/shard_map/rows/pallas_call | solution.py:414
  37.4 1.5 %collective-permute-start.11 = (f32[8,256]{1,0:T(8,128)S(1)}, f32[8,256]{1,0:T(8,128)S(1)}, u32[]{:S(2)}, u32[]{:S(2)}) collective-permute-start(f32[8,256]{1,0:T(8,128)S(1)} %get-tuple-element.63.refs_0_), channel_id=1, source_target_pairs={{0,4},{4,0},{8,12},{12,8},{16,20},{20,16},{24,28},{28,24},{1,5},{5... | collective-permute-start | bytes 24584 | tf_op jit(solution)/shard_map/ppermute | solution.py:119
  39.0 2.2 %collective-permute-done.11.refs_1_ = f32[8,256]{1,0:T(8,128)S(1)} collective-permute-done((f32[8,256]{1,0:T(8,128)S(1)}, f32[8,256]{1,0:T(8,128)S(1)}, u32[]{:S(2)}, u32[]{:S(2)}) %collective-permute-start.11) | collective-permute-done | bytes 8224 | tf_op jit(solution)/shard_map/ppermute | solution.py:119
  41.1 0.1 merge.2.refs_0_
  41.3 1.6 %collective-permute-start.12 = (f32[8,256]{1,0:T(8,128)S(1)}, f32[8,256]{1,0:T(8,128)S(1)}, u32[]{:S(2)}, u32[]{:S(2)}) collective-permute-start(f32[8,256]{1,0:T(8,128)S(1)} %merge.2.refs_0_), channel_id=1, source_target_pairs={{0,8},{4,12},{8,0},{12,4},{16,24},{20,28},{24,16},{28,20},{1,9},{5... | collective-permute-start | bytes 24584 | tf_op jit(solution)/shard_map/ppermute | solution.py:119
  42.9 2.1 %collective-permute-done.12.refs_1_ = f32[8,256]{1,0:T(8,128)S(1)} collective-permute-done((f32[8,256]{1,0:T(8,128)S(1)}, f32[8,256]{1,0:T(8,128)S(1)}, u32[]{:S(2)}, u32[]{:S(2)}) %collective-permute-start.12) | collective-permute-done | bytes 8224 | tf_op jit(solution)/shard_map/ppermute | solution.py:119
  44.9 0.1 merge.3.refs_0_
  45.1 2.6 %collective-permute-start.13 = (f32[8,256]{1,0:T(8,128)S(1)}, f32[8,256]{1,0:T(8,128)S(1)}, u32[]{:S(2)}, u32[]{:S(2)}) collective-permute-start(f32[8,256]{1,0:T(8,128)S(1)} %merge.3.refs_0_), channel_id=1, source_target_pairs={{0,16},{4,20},{8,24},{12,28},{16,0},{20,4},{24,8},{28,12},{1,17},{... | collective-permute-start | bytes 24584 | tf_op jit(solution)/shard_map/ppermute | solution.py:119
  47.7 0.8 %flush.1 = (bf16[1024,512]{1,0:T(8,128)(2,1)}, bf16[1024,1024]{1,0:T(8,128)(2,1)}) custom-call(bf16[128,1536]{1,0:T(8,128)(2,1)S(1)} %get-tuple-element.58.stage, bf16[1024,512]{1,0:T(8,128)(2,1)} %get-tuple-element.59.refs_0_, bf16[1024,1024]{1,0:T(8,128)(2,1)} %get-tuple-element.60.refs_1_), custom_call_target="tpu_custom_call", output_to_operand_aliasing={{0}: (1, {}), {1}: (2, {})} | custom-call | flops 1000000 | bytes 1000000 | tf_op jit(solution)/shard_map/flush/pallas_call | solution.py:460
  48.5 1.2 %collective-permute-done.13.refs_1_ = f32[8,256]{1,0:T(8,128)S(1)} collective-permute-done((f32[8,256]{1,0:T(8,128)S(1)}, f32[8,256]{1,0:T(8,128)S(1)}, u32[]{:S(2)}, u32[]{:S(2)}) %collective-permute-start.13) | collective-permute-done | bytes 8224 | tf_op jit(solution)/shard_map/ppermute | solution.py:119
  49.6 1.0 %finish.1 = (f32[8,1024]{1,0:T(8,128)}, f32[8,128]{1,0:T(8,128)}) custom-call(f32[8,256]{1,0:T(8,128)S(1)} %merge.3.refs_0_, f32[8,256]{1,0:T(8,128)S(1)} %collective-permute-done.13.refs_1_, f32[8,256]{1,0:T(8,128)S(1)} %get-tuple-element.64.refs_2_, f32[8,1024]{1,0:T(8,128)S(1)} %get-tuple-element.65.refs_3_), custom_call_target="tpu_custom_call" | custom-call | flops 1000000 | bytes 100000 | tf_op jit(solution)/shard_map/finish/pallas_call | solution.py:144
  (3 shorter events, 0.0 us)
Async XLA Ops:
  0.6 18.0 %copy-start.2 = (bf16[2048,32]{0,1:T(8,128)(2,1)S(1)}, bf16[2048,32]{0,1:T(8,128)(2,1)}, u32[]{:S(2)}) copy-start(bf16[2048,32]{0,1:T(8,128)(2,1)} %param.11) | copy-start | bytes 393220
  0.6 17.9 %copy-start.3 = (bf16[2048,32]{0,1:T(8,128)(2,1)S(1)}, bf16[2048,32]{0,1:T(8,128)(2,1)}, u32[]{:S(2)}) copy-start(bf16[2048,32]{0,1:T(8,128)(2,1)} %param.12) | copy-start | bytes 393220
  0.7 17.9 %copy-start = (bf16[2048,1024]{1,0:T(8,128)(2,1)S(1)}, bf16[2048,1024]{1,0:T(8,128)(2,1)}, u32[]{:S(2)}) copy-start(bf16[2048,1024]{1,0:T(8,128)(2,1)} %refs_5_.5) | copy-start | bytes 12582916
  0.7 17.9 %copy-start.1 = (bf16[2048,512]{1,0:T(8,128)(2,1)S(1)}, bf16[2048,512]{1,0:T(8,128)(2,1)}, u32[]{:S(2)}) copy-start(bf16[2048,512]{1,0:T(8,128)(2,1)} %refs_4_.3) | copy-start | bytes 6291460
  0.7 25.4 %collective-permute-start.10 = (bf16[256,2048]{1,0:T(8,128)(2,1)}, bf16[256,2048]{1,0:T(8,128)(2,1)S(1)}, u32[]{:S(2)}, u32[]{:S(2)}) collective-permute-start(bf16[256,2048]{1,0:T(8,128)(2,1)} %x_ref.1), channel_id=1, source_target_pairs={{0,1},{1,0},{2,3},{3,2},{4,5},{5,4},{6,7},{7,6},{8,9},{9,8},{10,11... | collective-permute-start | bytes 3145736 | tf_op jit(solution)/shard_map/ppermute | solution.py:499
  1.2 1.6 %copy-start.4 = (bf16[256,2048]{1,0:T(8,128)(2,1)S(1)}, bf16[256,2048]{1,0:T(8,128)(2,1)}, u32[]{:S(2)}) copy-start(bf16[256,2048]{1,0:T(8,128)(2,1)} %x_ref.1) | copy-start | bytes 3145732
  2.8 5.0 %copy-start.7 = (bf16[512]{0:T(512)(128)(2,1)S(1)}, bf16[512]{0:T(512)(128)(2,1)}, u32[]{:S(2)}) copy-start(bf16[512]{0:T(512)(128)(2,1)} %param.15) | copy-start | bytes 3076
  2.8 5.0 %copy-start.6 = (bf16[2048]{0:T(1024)(128)(2,1)S(1)}, bf16[2048]{0:T(1024)(128)(2,1)}, u32[]{:S(2)}) copy-start(bf16[2048]{0:T(1024)(128)(2,1)} %param.14) | copy-start | bytes 12292
  2.8 15.8 %copy-start.5 = (f32[32]{0:T(128)S(1)}, f32[32]{0:T(128)}, u32[]{:S(2)}) copy-start(f32[32]{0:T(128)} %param.13) | copy-start | bytes 388
  3.2 9.5 %collective-permute-start.7 = (bf16[64,2048]{1,0:T(8,128)(2,1)S(1)}, bf16[64,2048]{1,0:T(8,128)(2,1)S(1)}, u32[]{:S(2)}, u32[]{:S(2)}) collective-permute-start(bf16[64,2048]{1,0:T(8,128)(2,1)S(1)} %get-tuple-element.39.refs_1_), channel_id=1, source_target_pairs={{0,2},{1,3},{2,0},{3,1},{4,6},{5,7},{6,4},{7,5},{8,10},{9,11},{10,... | collective-permute-start | bytes 786440 | tf_op jit(solution)/shard_map/ppermute | solution.py:502
  5.6 12.7 %collective-permute-start.6 = (bf16[64,2048]{1,0:T(8,128)(2,1)S(1)}, bf16[64,2048]{1,0:T(8,128)(2,1)S(1)}, u32[]{:S(2)}, u32[]{:S(2)}) collective-permute-start(bf16[64,2048]{1,0:T(8,128)(2,1)S(1)} %slice.3.refs_0_), channel_id=1, source_target_pairs={{0,2},{1,3},{2,0},{3,1},{4,6},{5,7},{6,4},{7,5},{8,10},{9,11},{10,... | collective-permute-start | bytes 786440 | tf_op jit(solution)/shard_map/ppermute | solution.py:502
  5.7 18.2 %collective-permute-start.4 = (bf16[64,2048]{1,0:T(8,128)(2,1)S(1)}, bf16[64,2048]{1,0:T(8,128)(2,1)S(1)}, u32[]{:S(2)}, u32[]{:S(2)}) collective-permute-start(bf16[64,2048]{1,0:T(8,128)(2,1)S(1)} %get-tuple-element.38.refs_2_), channel_id=1, source_target_pairs={{0,2},{1,3},{2,0},{3,1},{4,6},{5,7},{6,4},{7,5},{8,10},{9,11},{10,... | collective-permute-start | bytes 786440 | tf_op jit(solution)/shard_map/ppermute | solution.py:502
  7.7 21.5 %collective-permute-start = (bf16[48,2048]{1,0:T(8,128)(2,1)S(1)}, bf16[48,2048]{1,0:T(8,128)(2,1)S(1)}, u32[]{:S(2)}, u32[]{:S(2)}) collective-permute-start(bf16[48,2048]{1,0:T(8,128)(2,1)S(1)} %get-tuple-element.36.refs_3_), channel_id=1, source_target_pairs={{0,2},{1,3},{2,0},{3,1},{4,6},{5,7},{6,4},{7,5},{8,10},{9,11},{10,... | collective-permute-start | bytes 589832 | tf_op jit(solution)/shard_map/ppermute | solution.py:502
  12.7 16.9 %collective-permute-start.9 = (bf16[64,2048]{1,0:T(8,128)(2,1)S(1)}, bf16[64,2048]{1,0:T(8,128)(2,1)S(1)}, u32[]{:S(2)}, u32[]{:S(2)}) collective-permute-start(bf16[64,2048]{1,0:T(8,128)(2,1)S(1)} %collective-permute-done.7.refs_1_), channel_id=1, source_target_pairs={{0,1},{1,0},{2,3},{3,2},{4,5},{5,4},{6,7},{7,6},{8,9},{9,8},{10,11... | collective-permute-start | bytes 786440 | tf_op jit(solution)/shard_map/ppermute | solution.py:499
  18.3 12.1 %collective-permute-start.8 = (bf16[64,2048]{1,0:T(8,128)(2,1)S(1)}, bf16[64,2048]{1,0:T(8,128)(2,1)S(1)}, u32[]{:S(2)}, u32[]{:S(2)}) collective-permute-start(bf16[64,2048]{1,0:T(8,128)(2,1)S(1)} %collective-permute-done.6.refs_0_), channel_id=1, source_target_pairs={{0,1},{1,0},{2,3},{3,2},{4,5},{5,4},{6,7},{7,6},{8,9},{9,8},{10,11... | collective-permute-start | bytes 786440 | tf_op jit(solution)/shard_map/ppermute | solution.py:499
  23.9 11.8 %collective-permute-start.1 = (bf16[16,2048]{1,0:T(8,128)(2,1)S(1)}, bf16[16,2048]{1,0:T(8,128)(2,1)S(1)}, u32[]{:S(2)}, u32[]{:S(2)}) collective-permute-start(bf16[16,2048]{1,0:T(8,128)(2,1)S(1)} %get-tuple-element.37.refs_4_), channel_id=1, source_target_pairs={{0,2},{1,3},{2,0},{3,1},{4,6},{5,7},{6,4},{7,5},{8,10},{9,11},{10,... | collective-permute-start | bytes 196616 | tf_op jit(solution)/shard_map/ppermute | solution.py:502
  26.0 7.5 %collective-permute-start.5 = (bf16[64,2048]{1,0:T(8,128)(2,1)S(1)}, bf16[64,2048]{1,0:T(8,128)(2,1)S(1)}, u32[]{:S(2)}, u32[]{:S(2)}) collective-permute-start(bf16[64,2048]{1,0:T(8,128)(2,1)S(1)} %collective-permute-done.4.refs_0_), channel_id=1, source_target_pairs={{0,1},{1,0},{2,3},{3,2},{4,5},{5,4},{6,7},{7,6},{8,9},{9,8},{10,11... | collective-permute-start | bytes 786440 | tf_op jit(solution)/shard_map/ppermute | solution.py:499
  29.2 6.5 %collective-permute-start.3 = (bf16[16,2048]{1,0:T(8,128)(2,1)S(1)}, bf16[16,2048]{1,0:T(8,128)(2,1)S(1)}, u32[]{:S(2)}, u32[]{:S(2)}) collective-permute-start(bf16[16,2048]{1,0:T(8,128)(2,1)S(1)} %get-tuple-element.37.refs_4_), channel_id=1, source_target_pairs={{0,3},{1,2},{2,1},{3,0},{4,7},{5,6},{6,5},{7,4},{8,11},{9,10},{10,... | collective-permute-start | bytes 196616 | tf_op jit(solution)/shard_map/ppermute | solution.py:502
  29.6 6.2 %collective-permute-start.2 = (bf16[48,2048]{1,0:T(8,128)(2,1)S(1)}, bf16[48,2048]{1,0:T(8,128)(2,1)S(1)}, u32[]{:S(2)}, u32[]{:S(2)}) collective-permute-start(bf16[48,2048]{1,0:T(8,128)(2,1)S(1)} %collective-permute-done.refs_0_), channel_id=1, source_target_pairs={{0,1},{1,0},{2,3},{3,2},{4,5},{5,4},{6,7},{7,6},{8,9},{9,8},{10,11... | collective-permute-start | bytes 589832 | tf_op jit(solution)/shard_map/ppermute | solution.py:499
  37.4 3.7 %collective-permute-start.11 = (f32[8,256]{1,0:T(8,128)S(1)}, f32[8,256]{1,0:T(8,128)S(1)}, u32[]{:S(2)}, u32[]{:S(2)}) collective-permute-start(f32[8,256]{1,0:T(8,128)S(1)} %get-tuple-element.63.refs_0_), channel_id=1, source_target_pairs={{0,4},{4,0},{8,12},{12,8},{16,20},{20,16},{24,28},{28,24},{1,5},{5... | collective-permute-start | bytes 24584 | tf_op jit(solution)/shard_map/ppermute | solution.py:119
  41.3 3.7 %collective-permute-start.12 = (f32[8,256]{1,0:T(8,128)S(1)}, f32[8,256]{1,0:T(8,128)S(1)}, u32[]{:S(2)}, u32[]{:S(2)}) collective-permute-start(f32[8,256]{1,0:T(8,128)S(1)} %merge.2.refs_0_), channel_id=1, source_target_pairs={{0,8},{4,12},{8,0},{12,4},{16,24},{20,28},{24,16},{28,20},{1,9},{5... | collective-permute-start | bytes 24584 | tf_op jit(solution)/shard_map/ppermute | solution.py:119
  45.1 4.6 %collective-permute-start.13 = (f32[8,256]{1,0:T(8,128)S(1)}, f32[8,256]{1,0:T(8,128)S(1)}, u32[]{:S(2)}, u32[]{:S(2)}) collective-permute-start(f32[8,256]{1,0:T(8,128)S(1)} %merge.3.refs_0_), channel_id=1, source_target_pairs={{0,16},{4,20},{8,24},{12,28},{16,0},{20,4},{24,8},{28,12},{1,17},{... | collective-permute-start | bytes 24584 | tf_op jit(solution)/shard_map/ppermute | solution.py:119

commit v3 on v2

--- a/solution.py
+++ b/solution.py
@@ -470,8 +470,8 @@
     )(stage, *caches)
 
 
-UNITS = (4, 4, 4, 3, 1)
-TOGETHER = ((0, 1), (2,), (3, 4))
+UNITS = (7, 5, 3, 1)
+TOGETHER = ((0,), (1,), (2, 3))
 
 
 def body(
@@ -506,7 +506,7 @@
         )
 
     ahead = range(1, chips)
-    chunks = [prompt_tokens[: spans[0][1]], *cut(prompt_tokens, spans[1:])]
+    chunks = [prompt_tokens[a : a + size] for a, size in spans[:2]] + list(cut(prompt_tokens, spans[2:]))
     came = [[to_chip(v, d) for d in ahead] for v in chunks]
     crossed = [to_chip(chunks[-1], d, 1) for d in ahead]
     other = to_core(prompt_tokens)

time: 50.8 us -> 52.9 us (1.041)
  waiting for transfers between devices: 17.5 us -> 19.4 us
  local copies, waits for them, and re-layouts: 1.62 us -> 3.35 us
  starting transfers between devices: 14.6 us -> 13 us
    slice x1 -> x2, local copies, waits for them, and re-layouts: 0.02 us -> 2.08 us  [body(): prompt_tokens[a:a + size]]
    ppermute x6 -> x5, waiting for transfers between devices: 12.1 us -> 14 us  [to_chip(): lax.ppermute(v, 'tp', [(i, (i // 2 + ahead) % chips * 2 + i % 2 ^ flip) f...]
    ppermute x5 -> x4, starting transfers between devices: 1.91 us -> 0.29 us  [to_core(): return lax.ppermute(v, 'tp', [(i, i ^ 1) for i in range(devices)])]
    ppermute x6 -> x5, starting transfers between devices: 7.02 us -> 6.96 us  [to_chip(): lax.ppermute(v, 'tp', [(i, (i // 2 + ahead) % chips * 2 + i % 2 ^ flip) f...]
  transfers between devices with their start and end apart: 14 -> 12, of which waited for: 6 -> 6; matrix products, arithmetic and copies ran while one was open for 0% -> 2% of each run, Pallas kernels for 26% -> 25%
where the time goes in v3:
time: 52.9 us; the launch traced here: 52.7 us
  waiting for transfers between devices  19.4 us (37%)
  Pallas kernels  16.1 us (30%)
  starting transfers between devices  13 us (25%)
  local copies, waits for them, and re-layouts  3.35 us (6%)
  between operations  0.81 us (2%)
    ppermute x5, waiting for transfers between devices, to_chip(): lax.ppermute(v, 'tp', [(i, (i // 2 + ahead) % chips * 2 + i % 2 ^ flip) f...  14 us
    pallas_call x5, Pallas kernels, rows_call(): pl.pallas_call(functools.partial(rows_kernel, heads, places, len(xs), kin...  13.8 us
    ppermute x5, starting transfers between devices, to_chip(): lax.ppermute(v, 'tp', [(i, (i // 2 + ahead) % chips * 2 + i % 2 ^ flip) f...  6.96 us
    ppermute x3, starting transfers between devices, to_stage(): return lax.ppermute(message, 'sp', [(i, i ^ flip) for i in range(peers)])  5.71 us
    ppermute x3, waiting for transfers between devices, to_stage(): return lax.ppermute(message, 'sp', [(i, i ^ flip) for i in range(peers)])  5.41 us
    slice x2, local copies, waits for them, and re-layouts, body(): prompt_tokens[a:a + size]  2.08 us
    unnamed x16, local copies, waits for them, and re-layouts  1.26 us
  transfers between devices with their start and end apart: 12, of which 6 were waited for; matrix products, arithmetic and copies ran while one was open for 2% of the time, Pallas kernels for 25%

profile of v3, /device:TPU:0, one launch (start us, length us, event | category | flops | bytes accessed | tf_op | source)
XLA Modules:
  0.0 52.7 jit_solution(10473654121454461079)
XLA Ops:
  0.6 1.1 %slice.7.refs_0_ = bf16[112,2048]{1,0:T(8,128)(2,1)S(1)} slice(bf16[256,2048]{1,0:T(8,128)(2,1)} %x_ref.1), slice={[0:112], [0:2048]} | slice | bytes 917504 | tf_op jit(solution)/shard_map/slice | solution.py:509
  1.7 3.1 %collective-permute-start.6 = (bf16[112,2048]{1,0:T(8,128)(2,1)S(1)}, bf16[112,2048]{1,0:T(8,128)(2,1)S(1)}, u32[]{:S(2)}, u32[]{:S(2)}) collective-permute-start(bf16[112,2048]{1,0:T(8,128)(2,1)S(1)} %slice.7.refs_0_), channel_id=1, source_target_pairs={{0,2},{1,3},{2,0},{3,1},{4,6},{5,7},{6,4},{7,5},{8,10},{9,11},{10,... | collective-permute-start | bytes 1376264 | tf_op jit(solution)/shard_map/ppermute | solution.py:502
  4.7 0.0 collective-permute-start.8
  4.8 0.0 copy-start.7
  4.8 0.0 copy-start.6
  4.8 0.0 copy-start.5
  4.8 1.0 %slice.6.refs_1_ = bf16[80,2048]{1,0:T(8,128)(2,1)S(1)} slice(bf16[256,2048]{1,0:T(8,128)(2,1)} %x_ref.1), slice={[112:192], [0:2048]} | slice | bytes 655360 | tf_op jit(solution)/shard_map/slice | solution.py:509
  5.8 0.0 copy-start
  5.8 0.0 copy-start.1
  5.8 0.0 copy-start.2
  5.8 0.0 copy-start.3
  5.8 0.2 collective-permute-start.4
  6.0 10.1 %collective-permute-done.6.refs_0_ = bf16[112,2048]{1,0:T(8,128)(2,1)S(1)} collective-permute-done((bf16[112,2048]{1,0:T(8,128)(2,1)S(1)}, bf16[112,2048]{1,0:T(8,128)(2,1)S(1)}, u32[]{:S(2)}, u32[]{:S(2)}) %collective-permute-start.6) | collective-permute-done | bytes 458784 | tf_op jit(solution)/shard_map/ppermute | solution.py:502
  16.1 0.0 collective-permute-start.7
  16.1 0.0 copy-start.4
  16.1 1.2 %copy-done.4 = bf16[256,2048]{1,0:T(8,128)(2,1)S(1)} copy-done((bf16[256,2048]{1,0:T(8,128)(2,1)S(1)}, bf16[256,2048]{1,0:T(8,128)(2,1)}, u32[]{:S(2)}) %copy-start.4) | copy-done | bytes 1048600
  17.3 0.3 cut.1
  17.7 2.1 %collective-permute-start = (bf16[48,2048]{1,0:T(8,128)(2,1)S(1)}, bf16[48,2048]{1,0:T(8,128)(2,1)S(1)}, u32[]{:S(2)}, u32[]{:S(2)}) collective-permute-start(bf16[48,2048]{1,0:T(8,128)(2,1)S(1)} %get-tuple-element.34.refs_2_), channel_id=1, source_target_pairs={{0,2},{1,3},{2,0},{3,1},{4,6},{5,7},{6,4},{7,5},{8,10},{9,11},{10,... | collective-permute-start | bytes 589832 | tf_op jit(solution)/shard_map/ppermute | solution.py:502
  19.8 0.1 collective-permute-start.1
  19.8 0.0 copy-done.7
  19.9 0.0 copy-done.6
  19.9 3.3 %collective-permute-done.4.refs_0_ = bf16[80,2048]{1,0:T(8,128)(2,1)S(1)} collective-permute-done((bf16[80,2048]{1,0:T(8,128)(2,1)S(1)}, bf16[80,2048]{1,0:T(8,128)(2,1)S(1)}, u32[]{:S(2)}, u32[]{:S(2)}) %collective-permute-start.4) | collective-permute-done | bytes 327712 | tf_op jit(solution)/shard_map/ppermute | solution.py:502
  23.1 0.0 collective-permute-start.5
  23.1 0.0 copy-done.5
  23.1 0.0 copy-done
  23.1 0.0 copy-done.1
  23.2 0.0 copy-done.2
  23.2 0.0 copy-done.3
  23.2 3.4 %rows.5 = (bf16[1024,512]{1,0:T(8,128)(2,1)}, bf16[1024,1024]{1,0:T(8,128)(2,1)}, f32[8,256]{1,0:T(8,128)S(1)}, f32[8,256]{1,0:T(8,128)S(1)}, f32[8,256]{1,0:T(8,128)S(1)}) custom-call(bf16[112,2048]{1,0:T(8,128)(2,1)S(1)} %slice.7.refs_0_, bf16[80,2048]{1,0:T(8,128)(2,1)S(1)} %slice.6.refs_1_, bf16[48,2048]{1,0:T(8,128)(2,1)S(1)} %get-tuple-element.34.refs_2_, ...), custom_call_target="tpu_custom_call" | custom-call | flops 1711276032 | bytes 6291456 | tf_op jit(solution)/shard_map/rows/pallas_call | solution.py:414
  26.6 0.6 %collective-permute-done.refs_0_ = bf16[48,2048]{1,0:T(8,128)(2,1)S(1)} collective-permute-done((bf16[48,2048]{1,0:T(8,128)(2,1)S(1)}, bf16[48,2048]{1,0:T(8,128)(2,1)S(1)}, u32[]{:S(2)}, u32[]{:S(2)}) %collective-permute-start) | collective-permute-done | bytes 196640 | tf_op jit(solution)/shard_map/ppermute | solution.py:502
  27.2 1.6 %collective-permute-start.3 = (bf16[16,2048]{1,0:T(8,128)(2,1)S(1)}, bf16[16,2048]{1,0:T(8,128)(2,1)S(1)}, u32[]{:S(2)}, u32[]{:S(2)}) collective-permute-start(bf16[16,2048]{1,0:T(8,128)(2,1)S(1)} %get-tuple-element.35.refs_3_), channel_id=1, source_target_pairs={{0,3},{1,2},{2,1},{3,0},{4,7},{5,6},{6,5},{7,4},{8,11},{9,10},{10,... | collective-permute-start | bytes 196616 | tf_op jit(solution)/shard_map/ppermute | solution.py:502
  28.8 0.0 collective-permute-done.8.refs_0_
  28.8 0.3 collective-permute-start.2
  29.1 3.2 %rows.6 = (bf16[1024,512]{1,0:T(8,128)(2,1)}, bf16[1024,1024]{1,0:T(8,128)(2,1)}, f32[8,256]{1,0:T(8,128)S(1)}, f32[8,256]{1,0:T(8,128)S(1)}) custom-call(bf16[256,2048]{1,0:T(8,128)(2,1)S(1)} %collective-permute-done.8.refs_0_, bf16[2048,512]{1,0:T(8,128)(2,1)S(1)} %copy-done.1, ...), custom_call_target="tpu_custom_call", output_to_operand_aliasing={{0}: (7, {}), {1}: (8, {})} | custom-call | flops 1610612736 | bytes 6291456 | tf_op jit(solution)/shard_map/rows/pallas_call | solution.py:414
  32.2 0.0 collective-permute-done.7.refs_1_
  32.2 3.0 %rows.7 = (bf16[1024,512]{1,0:T(8,128)(2,1)}, bf16[1024,1024]{1,0:T(8,128)(2,1)}, f32[8,256]{1,0:T(8,128)S(1)}, f32[8,256]{1,0:T(8,128)S(1)}, f32[8,112]{1,0:T(8,128)S(1)}, /*index=5*/f32[8,112]{1,0:T(8,128)S(1)}) custom-call(bf16[112,2048]{1,0:T(8,128)(2,1)S(1)} %collective-permute-done.6.refs_0_, ...), custom_call_target="tpu_custom_call", output_to_operand_aliasing={{0}: (8, {}), {1}: (9, {})} | custom-call | flops 1409286144 | bytes 6291456 | tf_op jit(solution)/shard_map/rows/pallas_call | solution.py:414
  35.3 0.0 collective-permute-done.5.refs_1_
  35.3 2.5 %rows.8 = (bf16[1024,512]{1,0:T(8,128)(2,1)}, bf16[1024,1024]{1,0:T(8,128)(2,1)}, f32[8,256]{1,0:T(8,128)S(1)}, f32[8,256]{1,0:T(8,128)S(1)}, f32[8,192]{1,0:T(8,128)S(1)}, /*index=5*/f32[8,192]{1,0:T(8,128)S(1)}) custom-call(bf16[80,2048]{1,0:T(8,128)(2,1)S(1)} %collective-permute-done.4.refs_0_, ...), custom_call_target="tpu_custom_call", output_to_operand_aliasing={{0}: (12, {}), {1}: (13, {})} | custom-call | flops 1006632960 | bytes 6291456 | tf_op jit(solution)/shard_map/rows/pallas_call | solution.py:414
  37.8 0.0 collective-permute-done.1.refs_1_
  37.8 0.0 collective-permute-done.3.refs_3_
  37.8 0.0 collective-permute-done.2.refs_2_
  37.8 1.7 %rows.9 = (bf16[128,1536]{1,0:T(8,128)(2,1)S(1)}, f32[8,256]{1,0:T(8,128)S(1)}, f32[8,1024]{1,0:T(8,128)S(1)}) custom-call(bf16[48,2048]{1,0:T(8,128)(2,1)S(1)} %collective-permute-done.refs_0_, bf16[16,2048]{1,0:T(8,128)(2,1)S(1)} %collective-permute-done.1.refs_1_, bf16[48,2048]{1,0:T(8,128)(2,1)S(1)} %collective-permute-done.2.refs_2_, ...), custom_call_target="tpu_custom_call" | custom-call | flops 805306368 | bytes 6291456 | tf_op jit(solution)/shard_map/rows/pallas_call | solution.py:414
  39.5 1.5 %collective-permute-start.9 = (f32[8,256]{1,0:T(8,128)S(1)}, f32[8,256]{1,0:T(8,128)S(1)}, u32[]{:S(2)}, u32[]{:S(2)}) collective-permute-start(f32[8,256]{1,0:T(8,128)S(1)} %get-tuple-element.59.refs_0_), channel_id=1, source_target_pairs={{0,4},{4,0},{8,12},{12,8},{16,20},{20,16},{24,28},{28,24},{1,5},{5... | collective-permute-start | bytes 24584 | tf_op jit(solution)/shard_map/ppermute | solution.py:119
  41.0 2.2 %collective-permute-done.9.refs_1_ = f32[8,256]{1,0:T(8,128)S(1)} collective-permute-done((f32[8,256]{1,0:T(8,128)S(1)}, f32[8,256]{1,0:T(8,128)S(1)}, u32[]{:S(2)}, u32[]{:S(2)}) %collective-permute-start.9) | collective-permute-done | bytes 8224 | tf_op jit(solution)/shard_map/ppermute | solution.py:119
  43.2 0.1 merge.2.refs_0_
  43.3 1.6 %collective-permute-start.10 = (f32[8,256]{1,0:T(8,128)S(1)}, f32[8,256]{1,0:T(8,128)S(1)}, u32[]{:S(2)}, u32[]{:S(2)}) collective-permute-start(f32[8,256]{1,0:T(8,128)S(1)} %merge.2.refs_0_), channel_id=1, source_target_pairs={{0,8},{4,12},{8,0},{12,4},{16,24},{20,28},{24,16},{28,20},{1,9},{5... | collective-permute-start | bytes 24584 | tf_op jit(solution)/shard_map/ppermute | solution.py:119
  44.9 2.1 %collective-permute-done.10.refs_1_ = f32[8,256]{1,0:T(8,128)S(1)} collective-permute-done((f32[8,256]{1,0:T(8,128)S(1)}, f32[8,256]{1,0:T(8,128)S(1)}, u32[]{:S(2)}, u32[]{:S(2)}) %collective-permute-start.10) | collective-permute-done | bytes 8224 | tf_op jit(solution)/shard_map/ppermute | solution.py:119
  47.0 0.1 merge.3.refs_0_
  47.2 2.6 %collective-permute-start.11 = (f32[8,256]{1,0:T(8,128)S(1)}, f32[8,256]{1,0:T(8,128)S(1)}, u32[]{:S(2)}, u32[]{:S(2)}) collective-permute-start(f32[8,256]{1,0:T(8,128)S(1)} %merge.3.refs_0_), channel_id=1, source_target_pairs={{0,16},{4,20},{8,24},{12,28},{16,0},{20,4},{24,8},{28,12},{1,17},{... | collective-permute-start | bytes 24584 | tf_op jit(solution)/shard_map/ppermute | solution.py:119
  49.8 0.8 %flush.1 = (bf16[1024,512]{1,0:T(8,128)(2,1)}, bf16[1024,1024]{1,0:T(8,128)(2,1)}) custom-call(bf16[128,1536]{1,0:T(8,128)(2,1)S(1)} %get-tuple-element.54.stage, bf16[1024,512]{1,0:T(8,128)(2,1)} %get-tuple-element.55.refs_0_, bf16[1024,1024]{1,0:T(8,128)(2,1)} %get-tuple-element.56.refs_1_), custom_call_target="tpu_custom_call", output_to_operand_aliasing={{0}: (1, {}), {1}: (2, {})} | custom-call | flops 1000000 | bytes 1000000 | tf_op jit(solution)/shard_map/flush/pallas_call | solution.py:460
  50.5 1.2 %collective-permute-done.11.refs_1_ = f32[8,256]{1,0:T(8,128)S(1)} collective-permute-done((f32[8,256]{1,0:T(8,128)S(1)}, f32[8,256]{1,0:T(8,128)S(1)}, u32[]{:S(2)}, u32[]{:S(2)}) %collective-permute-start.11) | collective-permute-done | bytes 8224 | tf_op jit(solution)/shard_map/ppermute | solution.py:119
  51.7 1.0 %finish.1 = (f32[8,1024]{1,0:T(8,128)}, f32[8,128]{1,0:T(8,128)}) custom-call(f32[8,256]{1,0:T(8,128)S(1)} %merge.3.refs_0_, f32[8,256]{1,0:T(8,128)S(1)} %collective-permute-done.11.refs_1_, f32[8,256]{1,0:T(8,128)S(1)} %get-tuple-element.60.refs_2_, f32[8,1024]{1,0:T(8,128)S(1)} %get-tuple-element.61.refs_3_), custom_call_target="tpu_custom_call" | custom-call | flops 1000000 | bytes 100000 | tf_op jit(solution)/shard_map/finish/pallas_call | solution.py:144
  (2 shorter events, 0.0 us)
Async XLA Ops:
  1.7 14.4 %collective-permute-start.6 = (bf16[112,2048]{1,0:T(8,128)(2,1)S(1)}, bf16[112,2048]{1,0:T(8,128)(2,1)S(1)}, u32[]{:S(2)}, u32[]{:S(2)}) collective-permute-start(bf16[112,2048]{1,0:T(8,128)(2,1)S(1)} %slice.7.refs_0_), channel_id=1, source_target_pairs={{0,2},{1,3},{2,0},{3,1},{4,6},{5,7},{6,4},{7,5},{8,10},{9,11},{10,... | collective-permute-start | bytes 1376264 | tf_op jit(solution)/shard_map/ppermute | solution.py:502
  4.7 24.0 %collective-permute-start.8 = (bf16[256,2048]{1,0:T(8,128)(2,1)}, bf16[256,2048]{1,0:T(8,128)(2,1)S(1)}, u32[]{:S(2)}, u32[]{:S(2)}) collective-permute-start(bf16[256,2048]{1,0:T(8,128)(2,1)} %x_ref.1), channel_id=1, source_target_pairs={{0,1},{1,0},{2,3},{3,2},{4,5},{5,4},{6,7},{7,6},{8,9},{9,8},{10,11... | collective-permute-start | bytes 3145736 | tf_op jit(solution)/shard_map/ppermute | solution.py:499
  4.8 15.1 %copy-start.7 = (bf16[512]{0:T(512)(128)(2,1)S(1)}, bf16[512]{0:T(512)(128)(2,1)}, u32[]{:S(2)}) copy-start(bf16[512]{0:T(512)(128)(2,1)} %param.15) | copy-start | bytes 3076
  4.8 15.1 %copy-start.6 = (bf16[2048]{0:T(1024)(128)(2,1)S(1)}, bf16[2048]{0:T(1024)(128)(2,1)}, u32[]{:S(2)}) copy-start(bf16[2048]{0:T(1024)(128)(2,1)} %param.14) | copy-start | bytes 12292
  4.8 18.4 %copy-start.5 = (f32[32]{0:T(128)S(1)}, f32[32]{0:T(128)}, u32[]{:S(2)}) copy-start(f32[32]{0:T(128)} %param.13) | copy-start | bytes 388
  5.8 17.4 %copy-start = (bf16[2048,1024]{1,0:T(8,128)(2,1)S(1)}, bf16[2048,1024]{1,0:T(8,128)(2,1)}, u32[]{:S(2)}) copy-start(bf16[2048,1024]{1,0:T(8,128)(2,1)} %refs_5_.3) | copy-start | bytes 12582916
  5.8 17.3 %copy-start.1 = (bf16[2048,512]{1,0:T(8,128)(2,1)S(1)}, bf16[2048,512]{1,0:T(8,128)(2,1)}, u32[]{:S(2)}) copy-start(bf16[2048,512]{1,0:T(8,128)(2,1)} %refs_4_.3) | copy-start | bytes 6291460
  5.8 17.3 %copy-start.2 = (bf16[2048,32]{0,1:T(8,128)(2,1)S(1)}, bf16[2048,32]{0,1:T(8,128)(2,1)}, u32[]{:S(2)}) copy-start(bf16[2048,32]{0,1:T(8,128)(2,1)} %param.11) | copy-start | bytes 393220
  5.8 17.3 %copy-start.3 = (bf16[2048,32]{0,1:T(8,128)(2,1)S(1)}, bf16[2048,32]{0,1:T(8,128)(2,1)}, u32[]{:S(2)}) copy-start(bf16[2048,32]{0,1:T(8,128)(2,1)} %param.12) | copy-start | bytes 393220
  5.8 17.3 %collective-permute-start.4 = (bf16[80,2048]{1,0:T(8,128)(2,1)S(1)}, bf16[80,2048]{1,0:T(8,128)(2,1)S(1)}, u32[]{:S(2)}, u32[]{:S(2)}) collective-permute-start(bf16[80,2048]{1,0:T(8,128)(2,1)S(1)} %slice.6.refs_1_), channel_id=1, source_target_pairs={{0,2},{1,3},{2,0},{3,1},{4,6},{5,7},{6,4},{7,5},{8,10},{9,11},{10,... | collective-permute-start | bytes 983048 | tf_op jit(solution)/shard_map/ppermute | solution.py:502
  16.1 16.1 %collective-permute-start.7 = (bf16[112,2048]{1,0:T(8,128)(2,1)S(1)}, bf16[112,2048]{1,0:T(8,128)(2,1)S(1)}, u32[]{:S(2)}, u32[]{:S(2)}) collective-permute-start(bf16[112,2048]{1,0:T(8,128)(2,1)S(1)} %collective-permute-done.6.refs_0_), channel_id=1, source_target_pairs={{0,1},{1,0},{2,3},{3,2},{4,5},{5,4},{6,7},{7,6},{8,9},{9,8},{10,11... | collective-permute-start | bytes 1376264 | tf_op jit(solution)/shard_map/ppermute | solution.py:499
  16.1 1.2 %copy-start.4 = (bf16[256,2048]{1,0:T(8,128)(2,1)S(1)}, bf16[256,2048]{1,0:T(8,128)(2,1)}, u32[]{:S(2)}) copy-start(bf16[256,2048]{1,0:T(8,128)(2,1)} %x_ref.1) | copy-start | bytes 3145732
  17.7 9.5 %collective-permute-start = (bf16[48,2048]{1,0:T(8,128)(2,1)S(1)}, bf16[48,2048]{1,0:T(8,128)(2,1)S(1)}, u32[]{:S(2)}, u32[]{:S(2)}) collective-permute-start(bf16[48,2048]{1,0:T(8,128)(2,1)S(1)} %get-tuple-element.34.refs_2_), channel_id=1, source_target_pairs={{0,2},{1,3},{2,0},{3,1},{4,6},{5,7},{6,4},{7,5},{8,10},{9,11},{10,... | collective-permute-start | bytes 589832 | tf_op jit(solution)/shard_map/ppermute | solution.py:502
  19.8 18.0 %collective-permute-start.1 = (bf16[16,2048]{1,0:T(8,128)(2,1)S(1)}, bf16[16,2048]{1,0:T(8,128)(2,1)S(1)}, u32[]{:S(2)}, u32[]{:S(2)}) collective-permute-start(bf16[16,2048]{1,0:T(8,128)(2,1)S(1)} %get-tuple-element.35.refs_3_), channel_id=1, source_target_pairs={{0,2},{1,3},{2,0},{3,1},{4,6},{5,7},{6,4},{7,5},{8,10},{9,11},{10,... | collective-permute-start | bytes 196616 | tf_op jit(solution)/shard_map/ppermute | solution.py:502
  23.1 12.1 %collective-permute-start.5 = (bf16[80,2048]{1,0:T(8,128)(2,1)S(1)}, bf16[80,2048]{1,0:T(8,128)(2,1)S(1)}, u32[]{:S(2)}, u32[]{:S(2)}) collective-permute-start(bf16[80,2048]{1,0:T(8,128)(2,1)S(1)} %collective-permute-done.4.refs_0_), channel_id=1, source_target_pairs={{0,1},{1,0},{2,3},{3,2},{4,5},{5,4},{6,7},{7,6},{8,9},{9,8},{10,11... | collective-permute-start | bytes 983048 | tf_op jit(solution)/shard_map/ppermute | solution.py:499
  27.2 10.6 %collective-permute-start.3 = (bf16[16,2048]{1,0:T(8,128)(2,1)S(1)}, bf16[16,2048]{1,0:T(8,128)(2,1)S(1)}, u32[]{:S(2)}, u32[]{:S(2)}) collective-permute-start(bf16[16,2048]{1,0:T(8,128)(2,1)S(1)} %get-tuple-element.35.refs_3_), channel_id=1, source_target_pairs={{0,3},{1,2},{2,1},{3,0},{4,7},{5,6},{6,5},{7,4},{8,11},{9,10},{10,... | collective-permute-start | bytes 196616 | tf_op jit(solution)/shard_map/ppermute | solution.py:502
  28.8 9.0 %collective-permute-start.2 = (bf16[48,2048]{1,0:T(8,128)(2,1)S(1)}, bf16[48,2048]{1,0:T(8,128)(2,1)S(1)}, u32[]{:S(2)}, u32[]{:S(2)}) collective-permute-start(bf16[48,2048]{1,0:T(8,128)(2,1)S(1)} %collective-permute-done.refs_0_), channel_id=1, source_target_pairs={{0,1},{1,0},{2,3},{3,2},{4,5},{5,4},{6,7},{7,6},{8,9},{9,8},{10,11... | collective-permute-start | bytes 589832 | tf_op jit(solution)/shard_map/ppermute | solution.py:499
  39.5 3.7 %collective-permute-start.9 = (f32[8,256]{1,0:T(8,128)S(1)}, f32[8,256]{1,0:T(8,128)S(1)}, u32[]{:S(2)}, u32[]{:S(2)}) collective-permute-start(f32[8,256]{1,0:T(8,128)S(1)} %get-tuple-element.59.refs_0_), channel_id=1, source_target_pairs={{0,4},{4,0},{8,12},{12,8},{16,20},{20,16},{24,28},{28,24},{1,5},{5... | collective-permute-start | bytes 24584 | tf_op jit(solution)/shard_map/ppermute | solution.py:119
  43.3 3.7 %collective-permute-start.10 = (f32[8,256]{1,0:T(8,128)S(1)}, f32[8,256]{1,0:T(8,128)S(1)}, u32[]{:S(2)}, u32[]{:S(2)}) collective-permute-start(f32[8,256]{1,0:T(8,128)S(1)} %merge.2.refs_0_), channel_id=1, source_target_pairs={{0,8},{4,12},{8,0},{12,4},{16,24},{20,28},{24,16},{28,20},{1,9},{5... | collective-permute-start | bytes 24584 | tf_op jit(solution)/shard_map/ppermute | solution.py:119
  47.2 4.6 %collective-permute-start.11 = (f32[8,256]{1,0:T(8,128)S(1)}, f32[8,256]{1,0:T(8,128)S(1)}, u32[]{:S(2)}, u32[]{:S(2)}) collective-permute-start(f32[8,256]{1,0:T(8,128)S(1)} %merge.3.refs_0_), channel_id=1, source_target_pairs={{0,16},{4,20},{8,24},{12,28},{16,0},{20,4},{24,8},{28,12},{1,17},{... | collective-permute-start | bytes 24584 | tf_op jit(solution)/shard_map/ppermute | solution.py:119

commit v4 on v3

--- a/solution.py
+++ b/solution.py
@@ -63,8 +63,8 @@
 
 
 def merge(slots, mine, heads):
-    radix = slots.shape[0]
-    stats = [slots[k, :, DV:] for k in range(radix)]
+    radix = len(slots)
+    stats = [slot[:, DV:] for slot in slots]
     totals = [column(s, TOTAL) for s in stats]
     carry, total = carries(totals)
     peaks = [column(s, PEAK) + c for s, c in zip(stats, carry, strict=True)]
@@ -74,21 +74,26 @@
     after = jnp.zeros((heads, 1), F32)
     for k in range(radix):
         scale = jnp.exp(peaks[k] - peak)
-        numer = numer + scale * slots[k, :, :DV]
+        numer = numer + scale * slots[k][:, :DV]
         denom = denom + scale * column(stats[k], DENOM)
         after = after + jnp.where(mine == k, carry[k], 0.0)
     return numer, denom, total, peak, after
 
 
-def place(slots, message_refs, digit):
-    for k, ref in enumerate(message_refs):
-        slots[digit ^ k] = ref[...]
+def placed(message_refs, digit):
+    out = []
+    for at in range(len(message_refs)):
+        here = message_refs[0][...]
+        for k in range(1, len(message_refs)):
+            here = jnp.where((digit ^ k) == at, message_refs[k][...], here)
+        out.append(here)
+    return out
 
 
 def merge_kernel(heads, radix, stride, *refs):
-    message_refs, out_ref, slots = refs[:radix], refs[radix], refs[radix + 1]
+    message_refs, out_ref = refs[:radix], refs[radix]
     digit = lax.rem(lax.axis_index("sp") // stride, radix)
-    place(slots, message_refs, digit)
+    slots = placed(message_refs, digit)
     numer, denom, total, peak, after = merge(slots, digit, heads)
     carried = message_refs[0][:, DV + CARRIED : DV + CARRIED + 1] + after
     out_ref[:, :DV] = numer
@@ -99,9 +104,9 @@
 
 def finish_kernel(heads, radix, stride, *refs):
     message_refs = refs[:radix]
-    kept_ref, log_ref, weight_ref, reading_ref, slots = refs[radix:]
+    kept_ref, log_ref, weight_ref, reading_ref = refs[radix:]
     digit = lax.rem(lax.axis_index("sp") // stride, radix)
-    place(slots, message_refs, digit)
+    slots = placed(message_refs, digit)
     numer, denom, _, peak, after = merge(slots, digit, heads)
     carried = message_refs[0][:, DV + CARRIED : DV + CARRIED + 1] + after
     new = kept_ref[:, DV:]
@@ -120,7 +125,7 @@
 
 
 def exchange(message, kept, log_weight, peers):
-    heads, width = message.shape
+    heads, _ = message.shape
     radices, left = [], peers
     while left > 1:
         radices.append(2 if left % 2 == 0 else left)
@@ -128,14 +133,12 @@
     stride = 1
     for n, radix in enumerate(radices):
         others = [to_stage(message, k * stride, peers) for k in range(1, radix)]
-        slots = [pltpu.VMEM((radix, heads, width), F32)]
         if n < len(radices) - 1:
             message = pl.pallas_call(
                 functools.partial(merge_kernel, heads, radix, stride),
                 out_shape=jax.ShapeDtypeStruct(message.shape, F32),
                 in_specs=[vmem()] * radix,
                 out_specs=vmem(),
-                scratch_shapes=slots,
                 compiler_params=params(4),
                 cost_estimate=cost(1e6, 1e5),
                 name="merge",
@@ -149,7 +152,6 @@
                 ),
                 in_specs=[vmem()] * (radix + 2),
                 out_specs=(vmem(), vmem()),
-                scratch_shapes=slots,
                 compiler_params=params(4),
                 cost_estimate=cost(1e6, 1e5),
                 name="finish",
@@ -350,7 +352,9 @@
         slots[device, :, DV:] = lane_pack({TOTAL: whole, PEAK: top, DENOM: denom}, heads)
     devices = slots.shape[0]
     carry, _ = carries([slots[k, :, DV + TOTAL : DV + TOTAL + 1] for k in range(devices)])
-    numer, denom, whole, top, _ = merge(slots, 0, heads)
+    numer, denom, whole, top, _ = merge(
+        [slots[k] for k in range(devices)], 0, heads
+    )
     sent_ref[:, :DV] = numer
     sent_ref[:, DV:] = lane_pack(
         {TOTAL: whole, PEAK: top, DENOM: denom, CARRIED: jnp.zeros_like(whole)}, heads

time: 52.9 us -> 52.9 us (level)
  no operation moved by 1% of the time
where the time goes in v4:
time: 52.9 us; the launch traced here: 52.7 us
  waiting for transfers between devices  19.4 us (37%)
  Pallas kernels  16.1 us (30%)
  starting transfers between devices  13 us (25%)
  local copies, waits for them, and re-layouts  3.35 us (6%)
  between operations  0.81 us (2%)
    ppermute x5, waiting for transfers between devices, to_chip(): lax.ppermute(v, 'tp', [(i, (i // 2 + ahead) % chips * 2 + i % 2 ^ flip) f...  14 us
    pallas_call x5, Pallas kernels, rows_call(): pl.pallas_call(functools.partial(rows_kernel, heads, places, len(xs), kin...  13.8 us
    ppermute x5, starting transfers between devices, to_chip(): lax.ppermute(v, 'tp', [(i, (i // 2 + ahead) % chips * 2 + i % 2 ^ flip) f...  6.96 us
    ppermute x3, starting transfers between devices, to_stage(): return lax.ppermute(message, 'sp', [(i, i ^ flip) for i in range(peers)])  5.71 us
    ppermute x3, waiting for transfers between devices, to_stage(): return lax.ppermute(message, 'sp', [(i, i ^ flip) for i in range(peers)])  5.41 us
    slice x2, local copies, waits for them, and re-layouts, body(): prompt_tokens[a:a + size]  2.08 us
    unnamed x16, local copies, waits for them, and re-layouts  1.26 us
  transfers between devices with their start and end apart: 12, of which 6 were waited for; matrix products, arithmetic and copies ran while one was open for 2% of the time, Pallas kernels for 25%

profile of v4, /device:TPU:0, one launch (start us, length us, event | category | flops | bytes accessed | tf_op | source)
XLA Modules:
  0.0 52.7 jit_solution(11378408876279666421)
XLA Ops:
  0.6 1.1 %slice.7.refs_0_ = bf16[112,2048]{1,0:T(8,128)(2,1)S(1)} slice(bf16[256,2048]{1,0:T(8,128)(2,1)} %x_ref.1), slice={[0:112], [0:2048]} | slice | bytes 917504 | tf_op jit(solution)/shard_map/slice | solution.py:513
  1.7 3.1 %collective-permute-start.6 = (bf16[112,2048]{1,0:T(8,128)(2,1)S(1)}, bf16[112,2048]{1,0:T(8,128)(2,1)S(1)}, u32[]{:S(2)}, u32[]{:S(2)}) collective-permute-start(bf16[112,2048]{1,0:T(8,128)(2,1)S(1)} %slice.7.refs_0_), channel_id=1, source_target_pairs={{0,2},{1,3},{2,0},{3,1},{4,6},{5,7},{6,4},{7,5},{8,10},{9,11},{10,... | collective-permute-start | bytes 1376264 | tf_op jit(solution)/shard_map/ppermute | solution.py:506
  4.7 0.0 collective-permute-start.8
  4.8 0.0 copy-start.7
  4.8 0.0 copy-start.6
  4.8 0.0 copy-start.5
  4.8 1.0 %slice.6.refs_1_ = bf16[80,2048]{1,0:T(8,128)(2,1)S(1)} slice(bf16[256,2048]{1,0:T(8,128)(2,1)} %x_ref.1), slice={[112:192], [0:2048]} | slice | bytes 655360 | tf_op jit(solution)/shard_map/slice | solution.py:513
  5.8 0.0 copy-start
  5.8 0.0 copy-start.1
  5.8 0.0 copy-start.2
  5.8 0.0 copy-start.3
  5.8 0.2 collective-permute-start.4
  6.0 10.1 %collective-permute-done.6.refs_0_ = bf16[112,2048]{1,0:T(8,128)(2,1)S(1)} collective-permute-done((bf16[112,2048]{1,0:T(8,128)(2,1)S(1)}, bf16[112,2048]{1,0:T(8,128)(2,1)S(1)}, u32[]{:S(2)}, u32[]{:S(2)}) %collective-permute-start.6) | collective-permute-done | bytes 458784 | tf_op jit(solution)/shard_map/ppermute | solution.py:506
  16.1 0.0 collective-permute-start.7
  16.1 0.0 copy-start.4
  16.1 1.2 %copy-done.4 = bf16[256,2048]{1,0:T(8,128)(2,1)S(1)} copy-done((bf16[256,2048]{1,0:T(8,128)(2,1)S(1)}, bf16[256,2048]{1,0:T(8,128)(2,1)}, u32[]{:S(2)}) %copy-start.4) | copy-done | bytes 1048600
  17.3 0.3 cut.1
  17.7 2.1 %collective-permute-start = (bf16[48,2048]{1,0:T(8,128)(2,1)S(1)}, bf16[48,2048]{1,0:T(8,128)(2,1)S(1)}, u32[]{:S(2)}, u32[]{:S(2)}) collective-permute-start(bf16[48,2048]{1,0:T(8,128)(2,1)S(1)} %get-tuple-element.34.refs_2_), channel_id=1, source_target_pairs={{0,2},{1,3},{2,0},{3,1},{4,6},{5,7},{6,4},{7,5},{8,10},{9,11},{10,... | collective-permute-start | bytes 589832 | tf_op jit(solution)/shard_map/ppermute | solution.py:506
  19.8 0.1 collective-permute-start.1
  19.8 0.0 copy-done.7
  19.9 0.0 copy-done.6
  19.9 3.3 %collective-permute-done.4.refs_0_ = bf16[80,2048]{1,0:T(8,128)(2,1)S(1)} collective-permute-done((bf16[80,2048]{1,0:T(8,128)(2,1)S(1)}, bf16[80,2048]{1,0:T(8,128)(2,1)S(1)}, u32[]{:S(2)}, u32[]{:S(2)}) %collective-permute-start.4) | collective-permute-done | bytes 327712 | tf_op jit(solution)/shard_map/ppermute | solution.py:506
  23.1 0.0 collective-permute-start.5
  23.1 0.0 copy-done.5
  23.1 0.0 copy-done
  23.1 0.0 copy-done.1
  23.2 0.0 copy-done.2
  23.2 0.0 copy-done.3
  23.2 3.4 %rows.5 = (bf16[1024,512]{1,0:T(8,128)(2,1)}, bf16[1024,1024]{1,0:T(8,128)(2,1)}, f32[8,256]{1,0:T(8,128)S(1)}, f32[8,256]{1,0:T(8,128)S(1)}, f32[8,256]{1,0:T(8,128)S(1)}) custom-call(bf16[112,2048]{1,0:T(8,128)(2,1)S(1)} %slice.7.refs_0_, bf16[80,2048]{1,0:T(8,128)(2,1)S(1)} %slice.6.refs_1_, bf16[48,2048]{1,0:T(8,128)(2,1)S(1)} %get-tuple-element.34.refs_2_, ...), custom_call_target="tpu_custom_call" | custom-call | flops 1711276032 | bytes 6291456 | tf_op jit(solution)/shard_map/rows/pallas_call | solution.py:418
  26.6 0.6 %collective-permute-done.refs_0_ = bf16[48,2048]{1,0:T(8,128)(2,1)S(1)} collective-permute-done((bf16[48,2048]{1,0:T(8,128)(2,1)S(1)}, bf16[48,2048]{1,0:T(8,128)(2,1)S(1)}, u32[]{:S(2)}, u32[]{:S(2)}) %collective-permute-start) | collective-permute-done | bytes 196640 | tf_op jit(solution)/shard_map/ppermute | solution.py:506
  27.2 1.6 %collective-permute-start.3 = (bf16[16,2048]{1,0:T(8,128)(2,1)S(1)}, bf16[16,2048]{1,0:T(8,128)(2,1)S(1)}, u32[]{:S(2)}, u32[]{:S(2)}) collective-permute-start(bf16[16,2048]{1,0:T(8,128)(2,1)S(1)} %get-tuple-element.35.refs_3_), channel_id=1, source_target_pairs={{0,3},{1,2},{2,1},{3,0},{4,7},{5,6},{6,5},{7,4},{8,11},{9,10},{10,... | collective-permute-start | bytes 196616 | tf_op jit(solution)/shard_map/ppermute | solution.py:506
  28.8 0.0 collective-permute-done.8.refs_0_
  28.8 0.3 collective-permute-start.2
  29.1 3.2 %rows.6 = (bf16[1024,512]{1,0:T(8,128)(2,1)}, bf16[1024,1024]{1,0:T(8,128)(2,1)}, f32[8,256]{1,0:T(8,128)S(1)}, f32[8,256]{1,0:T(8,128)S(1)}) custom-call(bf16[256,2048]{1,0:T(8,128)(2,1)S(1)} %collective-permute-done.8.refs_0_, bf16[2048,512]{1,0:T(8,128)(2,1)S(1)} %copy-done.1, ...), custom_call_target="tpu_custom_call", output_to_operand_aliasing={{0}: (7, {}), {1}: (8, {})} | custom-call | flops 1610612736 | bytes 6291456 | tf_op jit(solution)/shard_map/rows/pallas_call | solution.py:418
  32.2 0.0 collective-permute-done.7.refs_1_
  32.2 3.0 %rows.7 = (bf16[1024,512]{1,0:T(8,128)(2,1)}, bf16[1024,1024]{1,0:T(8,128)(2,1)}, f32[8,256]{1,0:T(8,128)S(1)}, f32[8,256]{1,0:T(8,128)S(1)}, f32[8,112]{1,0:T(8,128)S(1)}, /*index=5*/f32[8,112]{1,0:T(8,128)S(1)}) custom-call(bf16[112,2048]{1,0:T(8,128)(2,1)S(1)} %collective-permute-done.6.refs_0_, ...), custom_call_target="tpu_custom_call", output_to_operand_aliasing={{0}: (8, {}), {1}: (9, {})} | custom-call | flops 1409286144 | bytes 6291456 | tf_op jit(solution)/shard_map/rows/pallas_call | solution.py:418
  35.3 0.0 collective-permute-done.5.refs_1_
  35.3 2.5 %rows.8 = (bf16[1024,512]{1,0:T(8,128)(2,1)}, bf16[1024,1024]{1,0:T(8,128)(2,1)}, f32[8,256]{1,0:T(8,128)S(1)}, f32[8,256]{1,0:T(8,128)S(1)}, f32[8,192]{1,0:T(8,128)S(1)}, /*index=5*/f32[8,192]{1,0:T(8,128)S(1)}) custom-call(bf16[80,2048]{1,0:T(8,128)(2,1)S(1)} %collective-permute-done.4.refs_0_, ...), custom_call_target="tpu_custom_call", output_to_operand_aliasing={{0}: (12, {}), {1}: (13, {})} | custom-call | flops 1006632960 | bytes 6291456 | tf_op jit(solution)/shard_map/rows/pallas_call | solution.py:418
  37.8 0.0 collective-permute-done.1.refs_1_
  37.8 0.0 collective-permute-done.3.refs_3_
  37.8 0.0 collective-permute-done.2.refs_2_
  37.8 1.7 %rows.9 = (bf16[128,1536]{1,0:T(8,128)(2,1)S(1)}, f32[8,256]{1,0:T(8,128)S(1)}, f32[8,1024]{1,0:T(8,128)S(1)}) custom-call(bf16[48,2048]{1,0:T(8,128)(2,1)S(1)} %collective-permute-done.refs_0_, bf16[16,2048]{1,0:T(8,128)(2,1)S(1)} %collective-permute-done.1.refs_1_, bf16[48,2048]{1,0:T(8,128)(2,1)S(1)} %collective-permute-done.2.refs_2_, ...), custom_call_target="tpu_custom_call" | custom-call | flops 805306368 | bytes 6291456 | tf_op jit(solution)/shard_map/rows/pallas_call | solution.py:418
  39.5 1.5 %collective-permute-start.9 = (f32[8,256]{1,0:T(8,128)S(1)}, f32[8,256]{1,0:T(8,128)S(1)}, u32[]{:S(2)}, u32[]{:S(2)}) collective-permute-start(f32[8,256]{1,0:T(8,128)S(1)} %get-tuple-element.59.refs_0_), channel_id=1, source_target_pairs={{0,4},{4,0},{8,12},{12,8},{16,20},{20,16},{24,28},{28,24},{1,5},{5... | collective-permute-start | bytes 24584 | tf_op jit(solution)/shard_map/ppermute | solution.py:124
  41.0 2.2 %collective-permute-done.9.refs_1_ = f32[8,256]{1,0:T(8,128)S(1)} collective-permute-done((f32[8,256]{1,0:T(8,128)S(1)}, f32[8,256]{1,0:T(8,128)S(1)}, u32[]{:S(2)}, u32[]{:S(2)}) %collective-permute-start.9) | collective-permute-done | bytes 8224 | tf_op jit(solution)/shard_map/ppermute | solution.py:124
  43.2 0.1 merge.2.refs_0_
  43.3 1.6 %collective-permute-start.10 = (f32[8,256]{1,0:T(8,128)S(1)}, f32[8,256]{1,0:T(8,128)S(1)}, u32[]{:S(2)}, u32[]{:S(2)}) collective-permute-start(f32[8,256]{1,0:T(8,128)S(1)} %merge.2.refs_0_), channel_id=1, source_target_pairs={{0,8},{4,12},{8,0},{12,4},{16,24},{20,28},{24,16},{28,20},{1,9},{5... | collective-permute-start | bytes 24584 | tf_op jit(solution)/shard_map/ppermute | solution.py:124
  44.9 2.1 %collective-permute-done.10.refs_1_ = f32[8,256]{1,0:T(8,128)S(1)} collective-permute-done((f32[8,256]{1,0:T(8,128)S(1)}, f32[8,256]{1,0:T(8,128)S(1)}, u32[]{:S(2)}, u32[]{:S(2)}) %collective-permute-start.10) | collective-permute-done | bytes 8224 | tf_op jit(solution)/shard_map/ppermute | solution.py:124
  47.0 0.1 merge.3.refs_0_
  47.1 2.6 %collective-permute-start.11 = (f32[8,256]{1,0:T(8,128)S(1)}, f32[8,256]{1,0:T(8,128)S(1)}, u32[]{:S(2)}, u32[]{:S(2)}) collective-permute-start(f32[8,256]{1,0:T(8,128)S(1)} %merge.3.refs_0_), channel_id=1, source_target_pairs={{0,16},{4,20},{8,24},{12,28},{16,0},{20,4},{24,8},{28,12},{1,17},{... | collective-permute-start | bytes 24584 | tf_op jit(solution)/shard_map/ppermute | solution.py:124
  49.7 0.8 %flush.1 = (bf16[1024,512]{1,0:T(8,128)(2,1)}, bf16[1024,1024]{1,0:T(8,128)(2,1)}) custom-call(bf16[128,1536]{1,0:T(8,128)(2,1)S(1)} %get-tuple-element.54.stage, bf16[1024,512]{1,0:T(8,128)(2,1)} %get-tuple-element.55.refs_0_, bf16[1024,1024]{1,0:T(8,128)(2,1)} %get-tuple-element.56.refs_1_), custom_call_target="tpu_custom_call", output_to_operand_aliasing={{0}: (1, {}), {1}: (2, {})} | custom-call | flops 1000000 | bytes 1000000 | tf_op jit(solution)/shard_map/flush/pallas_call | solution.py:464
  50.5 1.2 %collective-permute-done.11.refs_1_ = f32[8,256]{1,0:T(8,128)S(1)} collective-permute-done((f32[8,256]{1,0:T(8,128)S(1)}, f32[8,256]{1,0:T(8,128)S(1)}, u32[]{:S(2)}, u32[]{:S(2)}) %collective-permute-start.11) | collective-permute-done | bytes 8224 | tf_op jit(solution)/shard_map/ppermute | solution.py:124
  51.7 1.0 %finish.1 = (f32[8,1024]{1,0:T(8,128)}, f32[8,128]{1,0:T(8,128)}) custom-call(f32[8,256]{1,0:T(8,128)S(1)} %merge.3.refs_0_, f32[8,256]{1,0:T(8,128)S(1)} %collective-permute-done.11.refs_1_, f32[8,256]{1,0:T(8,128)S(1)} %get-tuple-element.60.refs_2_, f32[8,1024]{1,0:T(8,128)S(1)} %get-tuple-element.61.refs_3_), custom_call_target="tpu_custom_call" | custom-call | flops 1000000 | bytes 100000 | tf_op jit(solution)/shard_map/finish/pallas_call | solution.py:147
  (2 shorter events, 0.0 us)
Async XLA Ops:
  1.7 14.4 %collective-permute-start.6 = (bf16[112,2048]{1,0:T(8,128)(2,1)S(1)}, bf16[112,2048]{1,0:T(8,128)(2,1)S(1)}, u32[]{:S(2)}, u32[]{:S(2)}) collective-permute-start(bf16[112,2048]{1,0:T(8,128)(2,1)S(1)} %slice.7.refs_0_), channel_id=1, source_target_pairs={{0,2},{1,3},{2,0},{3,1},{4,6},{5,7},{6,4},{7,5},{8,10},{9,11},{10,... | collective-permute-start | bytes 1376264 | tf_op jit(solution)/shard_map/ppermute | solution.py:506
  4.7 24.0 %collective-permute-start.8 = (bf16[256,2048]{1,0:T(8,128)(2,1)}, bf16[256,2048]{1,0:T(8,128)(2,1)S(1)}, u32[]{:S(2)}, u32[]{:S(2)}) collective-permute-start(bf16[256,2048]{1,0:T(8,128)(2,1)} %x_ref.1), channel_id=1, source_target_pairs={{0,1},{1,0},{2,3},{3,2},{4,5},{5,4},{6,7},{7,6},{8,9},{9,8},{10,11... | collective-permute-start | bytes 3145736 | tf_op jit(solution)/shard_map/ppermute | solution.py:503
  4.8 15.1 %copy-start.7 = (bf16[512]{0:T(512)(128)(2,1)S(1)}, bf16[512]{0:T(512)(128)(2,1)}, u32[]{:S(2)}) copy-start(bf16[512]{0:T(512)(128)(2,1)} %param.15) | copy-start | bytes 3076
  4.8 15.1 %copy-start.6 = (bf16[2048]{0:T(1024)(128)(2,1)S(1)}, bf16[2048]{0:T(1024)(128)(2,1)}, u32[]{:S(2)}) copy-start(bf16[2048]{0:T(1024)(128)(2,1)} %param.14) | copy-start | bytes 12292
  4.8 18.4 %copy-start.5 = (f32[32]{0:T(128)S(1)}, f32[32]{0:T(128)}, u32[]{:S(2)}) copy-start(f32[32]{0:T(128)} %param.13) | copy-start | bytes 388
  5.8 17.4 %copy-start = (bf16[2048,1024]{1,0:T(8,128)(2,1)S(1)}, bf16[2048,1024]{1,0:T(8,128)(2,1)}, u32[]{:S(2)}) copy-start(bf16[2048,1024]{1,0:T(8,128)(2,1)} %refs_5_.3) | copy-start | bytes 12582916
  5.8 17.3 %copy-start.1 = (bf16[2048,512]{1,0:T(8,128)(2,1)S(1)}, bf16[2048,512]{1,0:T(8,128)(2,1)}, u32[]{:S(2)}) copy-start(bf16[2048,512]{1,0:T(8,128)(2,1)} %refs_4_.3) | copy-start | bytes 6291460
  5.8 17.3 %copy-start.2 = (bf16[2048,32]{0,1:T(8,128)(2,1)S(1)}, bf16[2048,32]{0,1:T(8,128)(2,1)}, u32[]{:S(2)}) copy-start(bf16[2048,32]{0,1:T(8,128)(2,1)} %param.11) | copy-start | bytes 393220
  5.8 17.3 %copy-start.3 = (bf16[2048,32]{0,1:T(8,128)(2,1)S(1)}, bf16[2048,32]{0,1:T(8,128)(2,1)}, u32[]{:S(2)}) copy-start(bf16[2048,32]{0,1:T(8,128)(2,1)} %param.12) | copy-start | bytes 393220
  5.8 17.3 %collective-permute-start.4 = (bf16[80,2048]{1,0:T(8,128)(2,1)S(1)}, bf16[80,2048]{1,0:T(8,128)(2,1)S(1)}, u32[]{:S(2)}, u32[]{:S(2)}) collective-permute-start(bf16[80,2048]{1,0:T(8,128)(2,1)S(1)} %slice.6.refs_1_), channel_id=1, source_target_pairs={{0,2},{1,3},{2,0},{3,1},{4,6},{5,7},{6,4},{7,5},{8,10},{9,11},{10,... | collective-permute-start | bytes 983048 | tf_op jit(solution)/shard_map/ppermute | solution.py:506
  16.1 16.1 %collective-permute-start.7 = (bf16[112,2048]{1,0:T(8,128)(2,1)S(1)}, bf16[112,2048]{1,0:T(8,128)(2,1)S(1)}, u32[]{:S(2)}, u32[]{:S(2)}) collective-permute-start(bf16[112,2048]{1,0:T(8,128)(2,1)S(1)} %collective-permute-done.6.refs_0_), channel_id=1, source_target_pairs={{0,1},{1,0},{2,3},{3,2},{4,5},{5,4},{6,7},{7,6},{8,9},{9,8},{10,11... | collective-permute-start | bytes 1376264 | tf_op jit(solution)/shard_map/ppermute | solution.py:503
  16.1 1.2 %copy-start.4 = (bf16[256,2048]{1,0:T(8,128)(2,1)S(1)}, bf16[256,2048]{1,0:T(8,128)(2,1)}, u32[]{:S(2)}) copy-start(bf16[256,2048]{1,0:T(8,128)(2,1)} %x_ref.1) | copy-start | bytes 3145732
  17.7 9.5 %collective-permute-start = (bf16[48,2048]{1,0:T(8,128)(2,1)S(1)}, bf16[48,2048]{1,0:T(8,128)(2,1)S(1)}, u32[]{:S(2)}, u32[]{:S(2)}) collective-permute-start(bf16[48,2048]{1,0:T(8,128)(2,1)S(1)} %get-tuple-element.34.refs_2_), channel_id=1, source_target_pairs={{0,2},{1,3},{2,0},{3,1},{4,6},{5,7},{6,4},{7,5},{8,10},{9,11},{10,... | collective-permute-start | bytes 589832 | tf_op jit(solution)/shard_map/ppermute | solution.py:506
  19.8 18.0 %collective-permute-start.1 = (bf16[16,2048]{1,0:T(8,128)(2,1)S(1)}, bf16[16,2048]{1,0:T(8,128)(2,1)S(1)}, u32[]{:S(2)}, u32[]{:S(2)}) collective-permute-start(bf16[16,2048]{1,0:T(8,128)(2,1)S(1)} %get-tuple-element.35.refs_3_), channel_id=1, source_target_pairs={{0,2},{1,3},{2,0},{3,1},{4,6},{5,7},{6,4},{7,5},{8,10},{9,11},{10,... | collective-permute-start | bytes 196616 | tf_op jit(solution)/shard_map/ppermute | solution.py:506
  23.1 12.1 %collective-permute-start.5 = (bf16[80,2048]{1,0:T(8,128)(2,1)S(1)}, bf16[80,2048]{1,0:T(8,128)(2,1)S(1)}, u32[]{:S(2)}, u32[]{:S(2)}) collective-permute-start(bf16[80,2048]{1,0:T(8,128)(2,1)S(1)} %collective-permute-done.4.refs_0_), channel_id=1, source_target_pairs={{0,1},{1,0},{2,3},{3,2},{4,5},{5,4},{6,7},{7,6},{8,9},{9,8},{10,11... | collective-permute-start | bytes 983048 | tf_op jit(solution)/shard_map/ppermute | solution.py:503
  27.2 10.6 %collective-permute-start.3 = (bf16[16,2048]{1,0:T(8,128)(2,1)S(1)}, bf16[16,2048]{1,0:T(8,128)(2,1)S(1)}, u32[]{:S(2)}, u32[]{:S(2)}) collective-permute-start(bf16[16,2048]{1,0:T(8,128)(2,1)S(1)} %get-tuple-element.35.refs_3_), channel_id=1, source_target_pairs={{0,3},{1,2},{2,1},{3,0},{4,7},{5,6},{6,5},{7,4},{8,11},{9,10},{10,... | collective-permute-start | bytes 196616 | tf_op jit(solution)/shard_map/ppermute | solution.py:506
  28.8 9.0 %collective-permute-start.2 = (bf16[48,2048]{1,0:T(8,128)(2,1)S(1)}, bf16[48,2048]{1,0:T(8,128)(2,1)S(1)}, u32[]{:S(2)}, u32[]{:S(2)}) collective-permute-start(bf16[48,2048]{1,0:T(8,128)(2,1)S(1)} %collective-permute-done.refs_0_), channel_id=1, source_target_pairs={{0,1},{1,0},{2,3},{3,2},{4,5},{5,4},{6,7},{7,6},{8,9},{9,8},{10,11... | collective-permute-start | bytes 589832 | tf_op jit(solution)/shard_map/ppermute | solution.py:503
  39.5 3.7 %collective-permute-start.9 = (f32[8,256]{1,0:T(8,128)S(1)}, f32[8,256]{1,0:T(8,128)S(1)}, u32[]{:S(2)}, u32[]{:S(2)}) collective-permute-start(f32[8,256]{1,0:T(8,128)S(1)} %get-tuple-element.59.refs_0_), channel_id=1, source_target_pairs={{0,4},{4,0},{8,12},{12,8},{16,20},{20,16},{24,28},{28,24},{1,5},{5... | collective-permute-start | bytes 24584 | tf_op jit(solution)/shard_map/ppermute | solution.py:124
  43.3 3.7 %collective-permute-start.10 = (f32[8,256]{1,0:T(8,128)S(1)}, f32[8,256]{1,0:T(8,128)S(1)}, u32[]{:S(2)}, u32[]{:S(2)}) collective-permute-start(f32[8,256]{1,0:T(8,128)S(1)} %merge.2.refs_0_), channel_id=1, source_target_pairs={{0,8},{4,12},{8,0},{12,4},{16,24},{20,28},{24,16},{28,20},{1,9},{5... | collective-permute-start | bytes 24584 | tf_op jit(solution)/shard_map/ppermute | solution.py:124
  47.1 4.6 %collective-permute-start.11 = (f32[8,256]{1,0:T(8,128)S(1)}, f32[8,256]{1,0:T(8,128)S(1)}, u32[]{:S(2)}, u32[]{:S(2)}) collective-permute-start(f32[8,256]{1,0:T(8,128)S(1)} %merge.3.refs_0_), channel_id=1, source_target_pairs={{0,16},{4,20},{8,24},{12,28},{16,0},{20,4},{24,8},{28,12},{1,17},{... | collective-permute-start | bytes 24584 | tf_op jit(solution)/shard_map/ppermute | solution.py:124
